TPU v7x, 32 devices: a whole 2x2x4 slice. The times are simulated.
32 devices in a mesh: kv: 8 (over z, x), tp: 4 (over y, core).
Axes of the slice: x: 2, y: 2, z: 4, core: 2. Of those that a mesh axis runs over, the one named last changes fastest.
Arguments:
- tokens: bfloat16 [288, 4096], P(None, 'kv'), may hold values from -40 to 40
- norm_gain: float32 [4096], P('kv'), may hold values from 0.1 to 1.9
- query_weight: bfloat16 [4096, 2048], P('kv', 'tp'), may hold values from -0.09375 to 0.09375
- key_weight: bfloat16 [4096, 2048], P('kv', 'tp'), may hold values from -0.09375 to 0.09375
- value_weight: bfloat16 [4096, 2048], P('kv', 'tp'), may hold values from -0.09375 to 0.09375
- gate_weight: bfloat16 [4096, 32], replicated, may hold values from -0.09375 to 0.09375
- gate_bias: float32 [32], replicated, may hold values from -0.5 to 3
- out_weight: bfloat16 [2048, 4096], P('tp', 'kv'), may hold values from -0.125 to 0.125
- cache_keys: bfloat16 [12, 3072, 2048], P(None, 'kv', 'tp'), may hold values from -1000 to 1000
- cache_values: bfloat16 [12, 3072, 2048], P(None, 'kv', 'tp'), may hold values from -6 to 6
- cache_decay: float32 [12, 32, 3072], P(None, 'tp', 'kv'), may hold values from -3072 to 0, as said below
- lengths: int32 [12], replicated, may hold values from 1537 to 3072
- parents: int32 [12, 24], replicated, may hold values from 0 to 23, as said below
Outputs:
- mixed: bfloat16 [288, 4096], P('tp', 'kv')
Inputs may be any that keep to these rules, and one draw needn't show every extreme that they name: `cache_decay`: zero at and beyond lengths of the sequence. parents[s, 0] = 0 and parents[s, n] < n for n > 0.
All inputs are finite; a program needn't handle non-finite values.
Results may differ from a plain program's by a relative error of at most 0.014.
The roundings to bfloat16 on the way count: a program that leaves them out, or rounds other values in their place, can miss the bound.
Values may be sent and summed in bfloat16 or wider, within the bound.
A program may use at most 64 MiB of HBM per device.

v0:
```python
import functools

import jax
import jax.numpy as jnp
from jax import lax
from jax.experimental import pallas as pl
from jax.experimental.pallas import tpu as pltpu
from jax.sharding import PartitionSpec as P

F32 = jnp.float32
BF16 = jnp.bfloat16
LANES = 128
LOW = -1e30
NT = (((1,), (1,)), ((), ()))
HIGH = lax.Precision.HIGHEST


def dot(a, b, precision=None):
    return jnp.dot(a, b, preferred_element_type=F32, precision=precision)


def dot_nt(a, b, precision=None):
    return lax.dot_general(a, b, NT, preferred_element_type=F32, precision=precision)


def fold(x):
    half = x.shape[1] // 2
    return jnp.concatenate([x[:, :half], x[:, half:]], axis=0)


def unfold(x):
    rows = x.shape[0] // 2
    x = x.astype(F32)
    return jnp.concatenate([x[:rows], x[rows:]], axis=1)


def kernel(
    n,
    n_tp,
    tokens,
    gain,
    query_w,
    key_w,
    value_w,
    gate_hbm,
    bias,
    out_hbm,
    keys_hbm,
    values_hbm,
    decay,
    lengths,
    parents,
    out,
    part,
    part_v,
    pair_in,
    pair_in_v,
    part_in,
    part_in_v,
    gate_w,
    out_w,
    keys,
    values,
    qbuf,
    mix,
    stat,
    mix_in,
    stat_in,
    att,
    anc,
    path_s,
    tmix,
    tstat,
    kvnew,
    terms,
    terms_in,
    par_pad,
    load_sem,
    cache_sem,
    p_send,
    p_recv,
    a_send,
    a_recv,
    b_send,
    b_recv,
    c_send,
    c_recv,
    d_send,
    d_recv,
    e_send,
    e_recv,
):
    me = lax.axis_index("kv")
    tp = lax.axis_index("tp")
    rows, depth = tokens.shape
    seqs, props = parents.shape
    heads = decay.shape[1]
    pos_dev = keys.shape[1]
    width = query_w.shape[1]
    head_dim = width // heads
    scale = head_dim ** (-0.5)
    slots = part_in.shape[1]
    parity = lax.rem(tp, 2)
    left_over = seqs % n
    hp = heads * props

    barrier = pltpu.get_barrier_semaphore()
    for k in range(1, n):
        pl.semaphore_signal(barrier, inc=1, device_id={"kv": lax.rem(me + k, n)})
    for k in range(1, n_tp):
        pl.semaphore_signal(barrier, inc=1, device_id={"tp": lax.rem(tp + k, n_tp)})

    gate_load = pltpu.make_async_copy(
        gate_hbm.at[pl.ds(pl.multiple_of(me * depth, depth), depth), :], gate_w, load_sem.at[0]
    )
    gate_load.start()
    cache_loads = []
    for s in range(seqs):
        k_load = pltpu.make_async_copy(keys_hbm.at[s], keys.at[s], cache_sem.at[0, s])
        v_load = pltpu.make_async_copy(values_hbm.at[s], values.at[s], cache_sem.at[1, s])
        k_load.start()
        v_load.start()
        cache_loads.append((k_load, v_load))
    out_load = pltpu.make_async_copy(out_hbm, out_w, load_sem.at[1])
    out_load.start()

    def owner_of(s):
        if isinstance(s, int):
            place = s % n
            shift = parity * left_over if s // n == seqs // n else 0
        else:
            place = lax.rem(s, n)
            shift = jnp.where(lax.div(s, n) == seqs // n, parity * left_over, 0)
        return lax.rem(place + shift, n)

    def slot_seq(r):
        shift = parity * left_over if r == seqs // n else 0
        return r * n + lax.rem(me + 2 * n - shift, n)

    def for_slot(r, f):
        if (r + 1) * n <= seqs:
            f()
        else:
            pl.when(slot_seq(r) < seqs)(f)

    xf = tokens[...].astype(F32)
    squares = jnp.sum(xf * xf, axis=1, keepdims=True)
    normed = (xf * gain[...]).astype(BF16)
    sel_rows = lax.broadcasted_iota(jnp.int32, (bias.shape[1], LANES), 0)
    sel_cols = lax.broadcasted_iota(jnp.int32, (bias.shape[1], LANES), 1)
    select = ((sel_rows == sel_cols + tp * heads) & (sel_cols < heads)).astype(F32)
    for i, w in enumerate((query_w, key_w)):
        part[:, :, i * width : (i + 1) * width] = dot(normed, w[...]).reshape(seqs, props, width)
    value_part = dot(normed, value_w[...])
    for s in range(seqs):
        part_v[s] = fold(value_part[s * props : (s + 1) * props]).astype(BF16)
    gate_load.wait()
    gates_w = dot(gate_w[...], select.astype(BF16)).astype(BF16)
    gate_part = dot(normed, gates_w)
    lane = lax.broadcasted_iota(jnp.int32, (rows, LANES), 1)
    gate_part = jnp.where(lane == LANES // 2, squares, gate_part)
    part[:, :, 2 * width :] = gate_part.reshape(seqs, props, LANES)
    pl.semaphore_wait(barrier, n + n_tp - 2)

    side = lax.rem(me, 2)
    partner = me + 1 - 2 * side
    n_far = n // 2
    shares = ((part, pair_in, part_in), (part_v, pair_in_v, part_in_v))

    def p_copy(s, which):
        src, dst, _ = shares[which]
        return pltpu.make_async_remote_copy(
            src_ref=src.at[s],
            dst_ref=dst.at[s],
            send_sem=p_send.at[which, s],
            recv_sem=p_recv.at[which, s],
            device_id={"kv": partner},
        )

    def a_copy(s, which):
        src, _, dst = shares[which]
        d = owner_of(s)
        k = jnp.maximum(lax.rem(lax.div(me, 2) - lax.div(d, 2) + n_far, n_far) - 1, 0)
        return pltpu.make_async_remote_copy(
            src_ref=src.at[s],
            dst_ref=dst.at[k, s // n],
            send_sem=a_send.at[which, s],
            recv_sem=a_recv.at[which, k, s // n],
            device_id={"kv": d},
        )

    def crosses(s):
        return lax.rem(owner_of(s), 2) != side

    def passes(s):
        d = owner_of(s)
        return (lax.rem(d, 2) == side) & (d != me)

    for s in range(seqs):
        for which in range(2):
            pl.when(crosses(s))(p_copy(s, which).start)

    par_pad[...] = jnp.zeros(par_pad.shape, jnp.int32)
    par_pad[0:seqs, 0:props] = parents[...]
    r_i = lax.broadcasted_iota(jnp.int32, (LANES, LANES), 0)
    c_i = lax.broadcasted_iota(jnp.int32, (LANES, LANES), 1)
    eye = (r_i == c_i).astype(F32)
    bias_row = dot(jnp.broadcast_to(bias[...], (8, bias.shape[1])), select, HIGH)[0:1]

    def ancestry(r):
        s = slot_seq(r)
        row = par_pad[pl.ds(s, 1), :]
        link = jnp.maximum((row == r_i).astype(F32), eye).astype(BF16)
        for _ in range(props.bit_length()):
            link = jnp.minimum(dot(link, link), 1.0).astype(BF16)
        anc[r] = dot_nt(eye.astype(BF16), link)[:props]

    for r in range(slots):
        for_slot(r, functools.partial(ancestry, r))

    def pass_on(s):
        for which in range(2):
            p_copy(s, which).wait_recv()
        part[s] = part[s] + pair_in[s]
        part_v[s] = (part_v[s].astype(F32) + pair_in_v[s].astype(F32)).astype(BF16)
        for which in range(2):
            a_copy(s, which).start()

    for s in range(seqs):
        pl.when(passes(s))(functools.partial(pass_on, s))

    lane_p = lax.broadcasted_iota(jnp.int32, (props, LANES), 1)
    bd_row = lax.broadcasted_iota(jnp.int32, (heads, props, width), 0)
    bd_col = lax.broadcasted_iota(jnp.int32, (heads, props, width), 2)
    diag = (lax.div(bd_col, head_dim) == bd_row).reshape(hp, width)

    def spread(q):
        wide = jnp.broadcast_to(q[None], (heads, props, width)).reshape(hp, width)
        return jnp.where(diag, wide, 0.0).astype(BF16)

    def gather_diag(m):
        return jnp.sum(jnp.where(diag, m, 0.0).reshape(heads, props, width), axis=0)

    def to_lanes(col, first):
        acc = jnp.zeros((props, LANES), F32)
        for h in range(heads):
            acc = jnp.where(lane_p == h + first, col[h * props : (h + 1) * props], acc)
        return acc

    def b_copy(r, k, buf, send, recv):
        s = slot_seq(r)
        return pltpu.make_async_remote_copy(
            src_ref=buf.at[s],
            dst_ref=buf.at[s],
            send_sem=send.at[r, k - 1],
            recv_sem=recv.at[s],
            device_id={"kv": lax.rem(me + k, n)},
        )

    pad_rows = LANES - props

    def project(r):
        s = slot_seq(r)
        for which, (src, near, far) in enumerate(shares):
            pltpu.make_async_remote_copy(
                src_ref=src.at[0],
                dst_ref=near.at[s],
                send_sem=p_send.at[which, 0],
                recv_sem=p_recv.at[which, s],
                device_id={"kv": partner},
            ).wait_recv()
            for k in range(1, n_far):
                pltpu.make_async_remote_copy(
                    src_ref=src.at[0],
                    dst_ref=far.at[k - 1, r],
                    send_sem=a_send.at[which, 0],
                    recv_sem=a_recv.at[which, k - 1, r],
                    device_id={"kv": lax.rem(me + 2 * k, n)},
                ).wait_recv()
        total = part[s] + pair_in[s]
        total_v = unfold(part_v[s]) + unfold(pair_in_v[s])
        for k in range(1, n_far):
            total = total + part_in[k - 1, r]
            total_v = total_v + unfold(part_in_v[k - 1, r])
        tail = total[:, 2 * width :]
        square = jnp.sum(jnp.where(lane_p == LANES // 2, tail, 0.0), axis=1, keepdims=True)
        inverse = lax.rsqrt(square / (depth * n) + 1e-06)
        q = inverse * total[:, :width]
        qbuf[s] = fold(q).astype(BF16)
        for k in range(1, n):
            b_copy(r, k, qbuf, b_send, b_recv).start()
        kvnew[r, 0, 0:props] = inverse * total[:, width : 2 * width]
        kvnew[r, 1, 0:props] = inverse * total_v
        kvnew[r, :, props:] = jnp.zeros((2, pad_rows, width), F32)
        x = inverse * tail + bias_row
        log_gate = jnp.minimum(x, 0.0) - jnp.log1p(jnp.exp(-jnp.abs(x)))
        padded = jnp.concatenate([log_gate, jnp.zeros((pad_rows, LANES), F32)], axis=0)
        path_s[r] = dot(anc[r], padded, HIGH)

    def tree(r):
        s = slot_seq(r)
        path = path_s[r]
        q = spread(unfold(qbuf[s]))
        head_of = lax.broadcasted_iota(jnp.int32, (heads, props, LANES), 0)
        lane_of = lax.broadcasted_iota(jnp.int32, (heads, props, LANES), 2)
        pick = (head_of == lane_of).reshape(hp, LANES)
        tiled = jnp.broadcast_to(path[None], (heads, props, LANES)).reshape(hp, LANES)
        own = jnp.sum(jnp.where(pick, tiled, 0.0), axis=1, keepdims=True)
        padded = jnp.concatenate([path, jnp.zeros((pad_rows, LANES), F32)], axis=0)
        other = dot_nt(pick.astype(F32), padded, HIGH)
        scores = dot_nt(q, kvnew[r, 0].astype(BF16)) * scale + own - other
        live = jnp.broadcast_to(anc[r][None], (heads, props, LANES)).reshape(hp, LANES) > 0.5
        scores = jnp.where(live, scores, LOW)
        top = jnp.max(scores, axis=1, keepdims=True)
        w = jnp.where(live, jnp.exp(scores - top), 0.0)
        total = jnp.sum(w, axis=1, keepdims=True)
        tmix[r] = gather_diag(dot(w.astype(BF16), kvnew[r, 1].astype(BF16)))
        tstat[r, 0] = to_lanes(top, 0)
        tstat[r, 1] = to_lanes(total, 0)

    position = lax.broadcasted_iota(jnp.int32, (hp, pos_dev), 1) + me * pos_dev

    def c_copy(s, which, src, dst):
        d = owner_of(s)
        k = jnp.maximum(lax.rem(me - d + n, n) - 1, 0)
        slot = s // n if isinstance(s, int) else lax.div(s, n)
        return d, pltpu.make_async_remote_copy(
            src_ref=src.at[s],
            dst_ref=dst.at[k, slot],
            send_sem=c_send.at[which, s],
            recv_sem=c_recv.at[which, k, slot],
            device_id={"kv": d},
        )

    def shard(s, carry):
        d = owner_of(s)

        @pl.when(d != me)
        def _():
            pltpu.make_async_remote_copy(
                src_ref=qbuf.at[s],
                dst_ref=qbuf.at[s],
                send_sem=b_send.at[0, 0],
                recv_sem=b_recv.at[s],
                device_id={"kv": d},
            ).wait_recv()

        pltpu.make_async_copy(keys_hbm.at[s], keys.at[s], cache_sem.at[0, s]).wait()
        pltpu.make_async_copy(values_hbm.at[s], values.at[s], cache_sem.at[1, s]).wait()
        q = spread(unfold(qbuf[s]))
        fade = decay[s]
        fade = jnp.concatenate(
            [jnp.broadcast_to(fade[h : h + 1], (props, pos_dev)) for h in range(heads)], axis=0
        )
        scores = dot_nt(q, keys[s]) * scale + fade
        live = position < lengths[s]
        scores = jnp.where(live, scores, LOW)
        top = jnp.max(scores, axis=1, keepdims=True)
        w = jnp.where(live, jnp.exp(scores - top), 0.0)
        total = jnp.sum(w, axis=1, keepdims=True)
        mix[s] = fold(gather_diag(dot(w.astype(BF16), values[s]))).astype(BF16)
        stat[s] = to_lanes(top, 0) + to_lanes(total, heads)
        for which, (src, dst) in enumerate(((mix, mix_in), (stat, stat_in))):
            _, copy = c_copy(s, which, src, dst)
            pl.when(d != me)(copy.start)
        return carry

    ex_r = lax.broadcasted_iota(jnp.int32, (LANES, width), 0)
    ex_c = lax.broadcasted_iota(jnp.int32, (LANES, width), 1)
    widen = (ex_r == lax.div(ex_c, head_dim)).astype(F32)

    def merge(r):
        s = slot_seq(r)
        for k in range(1, n):
            for which, (src, dst) in enumerate(((mix, mix_in), (stat, stat_in))):
                pltpu.make_async_remote_copy(
                    src_ref=src.at[0],
                    dst_ref=dst.at[k - 1, r],
                    send_sem=c_send.at[which, 0],
                    recv_sem=c_recv.at[which, k - 1, r],
                    device_id={"kv": lax.rem(me + k, n)},
                ).wait_recv()
        stats = jnp.concatenate([stat[s]] + [stat_in[k, r] for k in range(n - 1)], axis=0)
        totals = pltpu.roll(stats, LANES - heads, 1).reshape(n, props, LANES)
        tops = stats.reshape(n, props, LANES) + path_s[r][None]
        tops = jnp.where((lane_p < heads)[None], tops, LOW)
        ttop = jnp.where(lane_p < heads, tstat[r, 0], LOW)
        best = jnp.maximum(jnp.max(tops, axis=0), ttop)
        factors = jnp.exp(tops - best[None])
        tfactor = jnp.exp(ttop - best)
        denom = jnp.sum(factors * totals, axis=0) + tfactor * tstat[r, 1]
        packed = jnp.concatenate([factors.reshape(n * props, LANES), tfactor, denom], axis=0)
        wide = dot(packed, widen, HIGH)
        numer = wide[n * props : (n + 1) * props] * tmix[r] + wide[:props] * unfold(mix[s])
        for k in range(1, n):
            numer = numer + wide[k * props : (k + 1) * props] * unfold(mix_in[k - 1, r])
        att[s] = fold(numer / wide[(n + 1) * props :]).astype(BF16)
        for k in range(1, n):
            b_copy(r, k, att, d_send, d_recv).start()

    for r in range(slots):
        for_slot(r, functools.partial(project, r))
        if r > 0:
            for_slot(r - 1, functools.partial(merge, r - 1))
        for_slot(r, functools.partial(tree, r))
        lax.fori_loop(r * n, min((r + 1) * n, seqs), shard, 0)
    for_slot(slots - 1, functools.partial(merge, slots - 1))

    out_load.wait()
    block = rows // n_tp

    def e_copy(t):
        k = lax.rem(tp - t + n_tp, n_tp)
        return pltpu.make_async_remote_copy(
            src_ref=terms.at[t],
            dst_ref=terms_in.at[jnp.maximum(k - 1, 0)],
            send_sem=e_send.at[t],
            recv_sem=e_recv.at[jnp.maximum(k - 1, 0)],
            device_id={"tp": t},
        )

    arrived = 0
    for t in range(n_tp):
        first, last = t * block // props, ((t + 1) * block - 1) // props + 1
        for s in range(arrived, last):
            d = owner_of(s)

            @pl.when(d != me)
            def _(s=s, d=d):
                pltpu.make_async_remote_copy(
                    src_ref=att.at[s],
                    dst_ref=att.at[s],
                    send_sem=d_send.at[0, 0],
                    recv_sem=d_recv.at[s],
                    device_id={"kv": d},
                ).wait_recv()

        arrived = max(arrived, last)
        attended = jnp.concatenate([unfold(att[s]) for s in range(first, last)], axis=0)
        term = dot(attended.astype(BF16), out_w[...])
        begin = t * block - first * props
        terms[t] = term[begin : begin + block].astype(BF16)
        pl.when(tp != t)(e_copy(t).start)
    total = terms[tp].astype(F32)
    for k in range(1, n_tp):
        pltpu.make_async_remote_copy(
            src_ref=terms.at[0],
            dst_ref=terms_in.at[k - 1],
            send_sem=e_send.at[0],
            recv_sem=e_recv.at[k - 1],
            device_id={"tp": lax.rem(tp + k, n_tp)},
        ).wait_recv()
        total = total + terms_in[k - 1].astype(F32)
    out[...] = total.astype(BF16)

    for s in range(seqs):
        d = owner_of(s)
        for which in range(2):
            pl.when(crosses(s))(p_copy(s, which).wait_send)
            pl.when(passes(s))(a_copy(s, which).wait_send)
        for which, (src, dst) in enumerate(((mix, mix_in), (stat, stat_in))):
            _, copy = c_copy(s, which, src, dst)
            pl.when(d != me)(copy.wait_send)
    for r in range(slots):

        def drain(r=r):
            for k in range(1, n):
                b_copy(r, k, qbuf, b_send, b_recv).wait_send()
                b_copy(r, k, att, d_send, d_recv).wait_send()

        for_slot(r, drain)
    for t in range(n_tp):
        pl.when(tp != t)(e_copy(t).wait_send)


def solution(mesh):
    n, n_tp = mesh.shape["kv"], mesh.shape["tp"]

    def body(
        tokens,
        norm_gain,
        query_weight,
        key_weight,
        value_weight,
        gate_weight,
        gate_bias,
        out_weight,
        cache_keys,
        cache_values,
        cache_decay,
        lengths,
        parents,
    ):
        rows, depth = tokens.shape
        seqs, props = parents.shape
        heads = cache_decay.shape[1]
        pos_dev = cache_keys.shape[1]
        width = query_weight.shape[1]
        cols = out_weight.shape[1]
        slots = -(-seqs // n)
        block = rows // n_tp
        all_w = 2 * width + LANES
        folded = (2 * props, width // 2)
        vmem = pl.BlockSpec(memory_space=pltpu.VMEM)
        hbm = pl.BlockSpec(memory_space=pl.ANY)
        smem = pl.BlockSpec(memory_space=pltpu.SMEM)
        dma = pltpu.SemaphoreType.DMA
        return pl.pallas_call(
            functools.partial(kernel, n, n_tp),
            out_shape=jax.ShapeDtypeStruct((block, cols), BF16),
            in_specs=[vmem, vmem, vmem, vmem, vmem, hbm, vmem, hbm, hbm, hbm, vmem, smem, vmem],
            out_specs=vmem,
            scratch_shapes=[
                pltpu.VMEM((seqs, props, all_w), F32),
                pltpu.VMEM((seqs,) + folded, BF16),
                pltpu.VMEM((seqs, props, all_w), F32),
                pltpu.VMEM((seqs,) + folded, BF16),
                pltpu.VMEM((n // 2 - 1, slots, props, all_w), F32),
                pltpu.VMEM((n // 2 - 1, slots) + folded, BF16),
                pltpu.VMEM((depth, gate_weight.shape[1]), BF16),
                pltpu.VMEM(out_weight.shape, BF16),
                pltpu.VMEM(cache_keys.shape, BF16),
                pltpu.VMEM(cache_values.shape, BF16),
                pltpu.VMEM((seqs,) + folded, BF16),
                pltpu.VMEM((seqs,) + folded, BF16),
                pltpu.VMEM((seqs, props, LANES), F32),
                pltpu.VMEM((n - 1, slots) + folded, BF16),
                pltpu.VMEM((n - 1, slots, props, LANES), F32),
                pltpu.VMEM((seqs,) + folded, BF16),
                pltpu.VMEM((slots, props, LANES), F32),
                pltpu.VMEM((slots, props, LANES), F32),
                pltpu.VMEM((slots, props, width), F32),
                pltpu.VMEM((slots, 2, props, LANES), F32),
                pltpu.VMEM((slots, 2, LANES, width), F32),
                pltpu.VMEM((n_tp, block, cols), BF16),
                pltpu.VMEM((n_tp - 1, block, cols), BF16),
                pltpu.VMEM((-(-seqs // 8) * 8, LANES), jnp.int32),
                dma((2,)),
                dma((2, seqs)),
                dma((2, seqs)),
                dma((2, seqs)),
                dma((2, seqs)),
                dma((2, n // 2 - 1, slots)),
                dma((slots, n - 1)),
                dma((seqs,)),
                dma((2, seqs)),
                dma((2, n - 1, slots)),
                dma((slots, n - 1)),
                dma((seqs,)),
                dma((n_tp,)),
                dma((n_tp - 1,)),
            ],
            compiler_params=pltpu.CompilerParams(
                collective_id=0, has_side_effects=True, vmem_limit_bytes=48 * 1024 * 1024
            ),
        )(
            tokens,
            norm_gain.reshape(1, depth),
            query_weight,
            key_weight,
            value_weight,
            gate_weight,
            gate_bias.reshape(1, gate_bias.shape[0]),
            out_weight,
            cache_keys,
            cache_values,
            cache_decay,
            lengths,
            parents,
        )

    in_specs = (
        P(None, "kv"),
        P("kv"),
        P("kv", "tp"),
        P("kv", "tp"),
        P("kv", "tp"),
        P(),
        P(),
        P("tp", "kv"),
        P(None, "kv", "tp"),
        P(None, "kv", "tp"),
        P(None, "tp", "kv"),
        P(),
        P(),
    )
    out_specs = P("tp", "kv")
    return jax.shard_map(body, mesh=mesh, in_specs=in_specs, out_specs=out_specs, check_vma=False)
```

profile of v0, /device:TPU:0, one launch (start us, length us, event | category | flops | bytes accessed | tf_op | source)
XLA Modules:
  0.0 76.9 jit_solution(6716129424910512477)
XLA Ops:
  0.0 1.4 %copy.14.gate_hbm = bf16[4096,32]{1,0:T(8,128)(2,1)S(1)} copy(bf16[4096,32]{0,1:T(8,128)(2,1)} %param.18) | data formatting | bytes 524288 | tf_op args[5]
  1.4 0.0 copy-start
  1.4 1.0 %copy-done = bf16[512,512]{1,0:T(8,128)(2,1)S(1)} copy-done((bf16[512,512]{1,0:T(8,128)(2,1)S(1)}, bf16[512,512]{1,0:T(8,128)(2,1)}, u32[]{:S(2)}) %copy-start) | copy-done | bytes 524312
  2.5 0.0 copy-start.1
  2.5 1.0 %copy-done.1 = bf16[512,512]{1,0:T(8,128)(2,1)S(1)} copy-done((bf16[512,512]{1,0:T(8,128)(2,1)S(1)}, bf16[512,512]{1,0:T(8,128)(2,1)}, u32[]{:S(2)}) %copy-start.1) | copy-done | bytes 524312
  3.5 0.0 copy-start.2
  3.5 1.0 %copy-done.2 = bf16[512,512]{1,0:T(8,128)(2,1)S(1)} copy-done((bf16[512,512]{1,0:T(8,128)(2,1)S(1)}, bf16[512,512]{1,0:T(8,128)(2,1)}, u32[]{:S(2)}) %copy-start.2) | copy-done | bytes 524312
  4.6 0.0 copy-start.3
  4.6 1.0 %copy-done.3 = bf16[512,512]{1,0:T(8,128)(2,1)S(1)} copy-done((bf16[512,512]{1,0:T(8,128)(2,1)S(1)}, bf16[512,512]{1,0:T(8,128)(2,1)}, u32[]{:S(2)}) %copy-start.3) | copy-done | bytes 524312
  5.6 0.0 copy-start.4
  5.6 1.0 %copy-done.4 = bf16[288,512]{1,0:T(8,128)(2,1)S(1)} copy-done((bf16[288,512]{1,0:T(8,128)(2,1)S(1)}, bf16[288,512]{1,0:T(8,128)(2,1)}, u32[]{:S(2)}) %copy-start.4) | copy-done | bytes 294936
  6.6 0.0 copy-start.5
  6.6 0.9 %copy-done.5 = f32[12,8,384]{2,1,0:T(8,128)S(1)} copy-done((f32[12,8,384]{2,1,0:T(8,128)S(1)}, f32[12,8,384]{2,1,0:T(8,128)}, u32[]{:S(2)}) %copy-start.5) | copy-done | bytes 147480
  7.5 0.0 copy-start.6
  7.5 0.7 copy-done.6
  8.2 0.0 copy-start.7
  8.2 0.7 copy-done.7
  8.9 0.0 copy-start.8
  8.9 0.7 copy-done.8
  9.5 0.0 copy-start.9
  9.5 0.7 copy-done.9
  10.2 66.1 %shard_map.127 = bf16[72,512]{1,0:T(8,128)(2,1)S(1)} custom-call(bf16[288,512]{1,0:T(8,128)(2,1)S(1)} %copy-done.4, f32[1,512]{1,0:T(1,128)S(1)} %bitcast.2, bf16[512,512]{1,0:T(8,128)(2,1)S(1)} %copy-done, bf16[512,512]{1,0:T(8,128)(2,1)S(1)} %copy-done.1, bf16[512,512]{1,0:T(8,128)(2,1)S(1)} %copy-done.2, bf16[4096,32]{1,0:T(8,128)(2,1)S(1)} %copy.14.gate_hbm, ...), custom_call_target="tpu_custom_call" | custom-call | tf_op jit(solution)/shard_map/pallas_call | solution.py:508
  76.3 0.6 copy.16
Async XLA Ops:
  1.4 1.0 %copy-start = (bf16[512,512]{1,0:T(8,128)(2,1)S(1)}, bf16[512,512]{1,0:T(8,128)(2,1)}, u32[]{:S(2)}) copy-start(bf16[512,512]{1,0:T(8,128)(2,1)} %query_w.1) | copy-start | bytes 1572868
  2.5 1.0 %copy-start.1 = (bf16[512,512]{1,0:T(8,128)(2,1)S(1)}, bf16[512,512]{1,0:T(8,128)(2,1)}, u32[]{:S(2)}) copy-start(bf16[512,512]{1,0:T(8,128)(2,1)} %key_w.1) | copy-start | bytes 1572868
  3.5 1.0 %copy-start.2 = (bf16[512,512]{1,0:T(8,128)(2,1)S(1)}, bf16[512,512]{1,0:T(8,128)(2,1)}, u32[]{:S(2)}) copy-start(bf16[512,512]{1,0:T(8,128)(2,1)} %value_w.1) | copy-start | bytes 1572868
  4.6 1.0 %copy-start.3 = (bf16[512,512]{1,0:T(8,128)(2,1)S(1)}, bf16[512,512]{1,0:T(8,128)(2,1)}, u32[]{:S(2)}) copy-start(bf16[512,512]{1,0:T(8,128)(2,1)} %out_hbm.1) | copy-start | bytes 1572868
  5.6 1.0 %copy-start.4 = (bf16[288,512]{1,0:T(8,128)(2,1)S(1)}, bf16[288,512]{1,0:T(8,128)(2,1)}, u32[]{:S(2)}) copy-start(bf16[288,512]{1,0:T(8,128)(2,1)} %tokens.1) | copy-start | bytes 884740
  6.6 0.9 %copy-start.5 = (f32[12,8,384]{2,1,0:T(8,128)S(1)}, f32[12,8,384]{2,1,0:T(8,128)}, u32[]{:S(2)}) copy-start(f32[12,8,384]{2,1,0:T(8,128)} %decay.1) | copy-start | bytes 442372
  7.5 0.7 copy-start.6
  8.2 0.7 copy-start.7
  8.9 0.7 copy-start.8
  9.5 0.7 copy-start.9
where the time goes:
time: 77.4 us; the launch traced here: 76.9 us
  Pallas kernels  66.1 us (85%)
  local copies, waits for them, and re-layouts  10.8 us (14%)
    pallas_call x1, Pallas kernels, body(): pl.pallas_call(functools.partial(kernel, n, n_tp), out_shape=jax.ShapeDty...  66.1 us
    unnamed x22, local copies, waits for them, and re-layouts  10.8 us

commit v1 on v0

--- a/solution.py
+++ b/solution.py
@@ -37,20 +37,30 @@
 def kernel(
     n,
     n_tp,
+    tokens_hbm,
+    gain_hbm,
+    query_hbm,
+    key_hbm,
+    value_hbm,
+    gate_hbm,
+    bias_hbm,
+    out_hbm,
+    keys_hbm,
+    values_hbm,
+    decay_hbm,
+    lengths_hbm,
+    parents_hbm,
+    out,
     tokens,
     gain,
     query_w,
     key_w,
     value_w,
-    gate_hbm,
     bias,
-    out_hbm,
-    keys_hbm,
-    values_hbm,
     decay,
     lengths,
     parents,
-    out,
+    small_sem,
     part,
     part_v,
     pair_in,
@@ -110,8 +120,24 @@
     for k in range(1, n_tp):
         pl.semaphore_signal(barrier, inc=1, device_id={"tp": lax.rem(tp + k, n_tp)})
 
+    pairs = (
+        (tokens_hbm, tokens),
+        (gain_hbm, gain),
+        (query_hbm, query_w),
+        (key_hbm, key_w),
+        (value_hbm, value_w),
+        (bias_hbm, bias),
+        (parents_hbm, parents),
+        (decay_hbm, decay),
+        (lengths_hbm, lengths),
+    )
+    small_loads = [
+        pltpu.make_async_copy(src, dst, small_sem.at[i]) for i, (src, dst) in enumerate(pairs)
+    ]
+    for load in small_loads:
+        load.start()
     gate_load = pltpu.make_async_copy(
-        gate_hbm.at[pl.ds(pl.multiple_of(me * depth, depth), depth), :], gate_w, load_sem.at[0]
+        gate_hbm.at[:, pl.ds(pl.multiple_of(me * depth, depth), depth)], gate_w, load_sem.at[0]
     )
     gate_load.start()
     cache_loads = []
@@ -143,6 +169,8 @@
         else:
             pl.when(slot_seq(r) < seqs)(f)
 
+    for load in small_loads:
+        load.wait()
     xf = tokens[...].astype(F32)
     squares = jnp.sum(xf * xf, axis=1, keepdims=True)
     normed = (xf * gain[...]).astype(BF16)
@@ -155,8 +183,10 @@
     for s in range(seqs):
         part_v[s] = fold(value_part[s * props : (s + 1) * props]).astype(BF16)
     gate_load.wait()
-    gates_w = dot(gate_w[...], select.astype(BF16)).astype(BF16)
-    gate_part = dot(normed, gates_w)
+    gates_w = lax.dot_general(
+        select.astype(BF16), gate_w[...], (((0,), (0,)), ((), ())), preferred_element_type=F32
+    )
+    gate_part = dot_nt(normed, gates_w.astype(BF16))
     lane = lax.broadcasted_iota(jnp.int32, (rows, LANES), 1)
     gate_part = jnp.where(lane == LANES // 2, squares, gate_part)
     part[:, :, 2 * width :] = gate_part.reshape(seqs, props, LANES)
@@ -502,22 +532,31 @@
         all_w = 2 * width + LANES
         folded = (2 * props, width // 2)
         vmem = pl.BlockSpec(memory_space=pltpu.VMEM)
-        hbm = pl.BlockSpec(memory_space=pl.ANY)
-        smem = pl.BlockSpec(memory_space=pltpu.SMEM)
+        hbm = pl.BlockSpec(memory_space=pltpu.HBM)
         dma = pltpu.SemaphoreType.DMA
         return pl.pallas_call(
             functools.partial(kernel, n, n_tp),
             out_shape=jax.ShapeDtypeStruct((block, cols), BF16),
-            in_specs=[vmem, vmem, vmem, vmem, vmem, hbm, vmem, hbm, hbm, hbm, vmem, smem, vmem],
+            in_specs=[hbm] * 13,
             out_specs=vmem,
             scratch_shapes=[
+                pltpu.VMEM(tokens.shape, BF16),
+                pltpu.VMEM((1, depth), F32),
+                pltpu.VMEM(query_weight.shape, BF16),
+                pltpu.VMEM(key_weight.shape, BF16),
+                pltpu.VMEM(value_weight.shape, BF16),
+                pltpu.VMEM((1, gate_bias.shape[0]), F32),
+                pltpu.VMEM(cache_decay.shape, F32),
+                pltpu.SMEM(lengths.shape, jnp.int32),
+                pltpu.VMEM(parents.shape, jnp.int32),
+                dma((9,)),
                 pltpu.VMEM((seqs, props, all_w), F32),
                 pltpu.VMEM((seqs,) + folded, BF16),
                 pltpu.VMEM((seqs, props, all_w), F32),
                 pltpu.VMEM((seqs,) + folded, BF16),
                 pltpu.VMEM((n // 2 - 1, slots, props, all_w), F32),
                 pltpu.VMEM((n // 2 - 1, slots) + folded, BF16),
-                pltpu.VMEM((depth, gate_weight.shape[1]), BF16),
+                pltpu.VMEM((gate_weight.shape[1], depth), BF16),
                 pltpu.VMEM(out_weight.shape, BF16),
                 pltpu.VMEM(cache_keys.shape, BF16),
                 pltpu.VMEM(cache_values.shape, BF16),
@@ -551,7 +590,7 @@
                 dma((n_tp - 1,)),
             ],
             compiler_params=pltpu.CompilerParams(
-                collective_id=0, has_side_effects=True, vmem_limit_bytes=48 * 1024 * 1024
+                collective_id=0, has_side_effects=True, vmem_limit_bytes=67_043_328
             ),
         )(
             tokens,
@@ -559,7 +598,7 @@
             query_weight,
             key_weight,
             value_weight,
-            gate_weight,
+            gate_weight.T,
             gate_bias.reshape(1, gate_bias.shape[0]),
             out_weight,
             cache_keys,

time: 77.4 us -> 70.1 us (0.906)
  local copies, waits for them, and re-layouts: 10.8 us -> 1.52 us
  Pallas kernels: 66.1 us -> 68.4 us
    unnamed x22 -> x1, local copies, waits for them, and re-layouts: 10.8 us -> 1.52 us
    pallas_call x1, Pallas kernels: 66.1 us -> 68.4 us  [body(): pl.pallas_call(functools.partial(kernel, n, n_tp), out_shape=jax.ShapeDty...]
where the time goes in v1:
time: 70.1 us; the launch traced here: 69.9 us
  Pallas kernels  68.4 us (98%)
  local copies, waits for them, and re-layouts  1.52 us (2%)
    pallas_call x1, Pallas kernels, body(): pl.pallas_call(functools.partial(kernel, n, n_tp), out_shape=jax.ShapeDty...  68.4 us
    unnamed x1, local copies, waits for them, and re-layouts  1.52 us

profile of v1, /device:TPU:0, one launch (start us, length us, event | category | flops | bytes accessed | tf_op | source)
XLA Modules:
  0.0 69.9 jit_solution(13215384206827777895)
XLA Ops:
  0.0 68.4 %shard_map.127 = bf16[72,512]{1,0:T(8,128)(2,1)} custom-call(bf16[288,512]{1,0:T(8,128)(2,1)} %tokens_hbm.1, f32[1,512]{1,0:T(1,128)} %bitcast.4, bf16[512,512]{1,0:T(8,128)(2,1)} %query_hbm.1, bf16[512,512]{1,0:T(8,128)(2,1)} %key_hbm.1, bf16[512,512]{1,0:T(8,128)(2,1)} %value_hbm.1, bf16[32,4096]{1,0:T(8,128)(2,1)} %bitcast.3, f32[1,32]{1,0:T(1,128)} %bitcast.5, ...), custom_call_target="tpu_custom_call" | custom-call | tf_op jit(solution)/shard_map/pallas_call | solution.py:537
  68.4 1.5 %copy.15 = bf16[72,512]{1,0:T(8,128)(2,1)} copy(bf16[72,512]{1,0:T(8,128)(2,1)} %shard_map.127) | data formatting | bytes 147456

commit v2 on v1

--- a/solution.py
+++ b/solution.py
@@ -1,4 +1,5 @@
 import functools
+import math
 
 import jax
 import jax.numpy as jnp
@@ -34,7 +35,7 @@
     return jnp.concatenate([x[:rows], x[rows:]], axis=1)
 
 
-def kernel(
+def by_sequence(
     n,
     n_tp,
     tokens_hbm,
@@ -503,6 +504,539 @@
         pl.when(tp != t)(e_copy(t).wait_send)
 
 
+def split3(x):
+    high = x.astype(BF16)
+    rest = x - high.astype(F32)
+    mid = rest.astype(BF16)
+    low = (rest - mid.astype(F32)).astype(BF16)
+    return high, mid, low
+
+
+def tile_rows(rows, total):
+    return jnp.concatenate([rows, jnp.zeros((total - rows.shape[0], rows.shape[1]), rows.dtype)], axis=0)
+
+
+def by_heads(
+    n,
+    n_tp,
+    wave,
+    tokens_hbm,
+    gain_hbm,
+    query_hbm,
+    key_hbm,
+    value_hbm,
+    gate_hbm,
+    bias_hbm,
+    out_hbm,
+    keys_hbm,
+    values_hbm,
+    decay_hbm,
+    lengths_hbm,
+    parents_hbm,
+    out,
+    tokens,
+    gain,
+    query_w,
+    key_w,
+    value_w,
+    gate_w,
+    bias,
+    decay,
+    lengths,
+    parents,
+    out_w,
+    keys,
+    values,
+    feats,
+    q_out,
+    q_in,
+    q_own,
+    q_far,
+    kv_out,
+    kv_in,
+    kv_own,
+    kv_pass,
+    kv_far,
+    qbuf,
+    mix,
+    mix_in,
+    stat,
+    stat_in,
+    att,
+    terms,
+    terms_in,
+    par_pad,
+    link_s,
+    anc_s,
+    path_s,
+    inv_s,
+    tmix,
+    tstat,
+    widen,
+    load_sem,
+    cache_sem,
+    qx_send,
+    qx_recv,
+    kx_send,
+    kx_recv,
+    qz_send,
+    qz_recv,
+    kz_send,
+    kz_recv,
+    b_send,
+    b_recv,
+    c_send,
+    c_recv,
+    d_send,
+    d_recv,
+    e_send,
+    e_recv,
+):
+    me = lax.axis_index("kv")
+    tp = lax.axis_index("tp")
+    side = lax.rem(me, 2)
+    far = lax.div(me, 2)
+    n_far = n // 2
+    rows, depth = tokens.shape
+    seqs, props = parents.shape
+    heads = decay.shape[1]
+    pos_dev = keys.shape[1]
+    width = query_w.shape[1]
+    head_dim = width // heads
+    scale = head_dim ** (-0.5)
+    exact_scale = math.frexp(scale)[0] == 0.5
+    own_heads = heads // n_far
+    cols = width // n_far
+    half_seqs = seqs // 2
+    half = rows // 2
+    waves = half_seqs // wave
+    wrows = wave * props
+    sources = n - 1
+
+    barrier = pltpu.get_barrier_semaphore()
+    for k in range(1, n):
+        pl.semaphore_signal(barrier, inc=1, device_id={"kv": lax.rem(me + k, n)})
+    for k in range(1, n_tp):
+        pl.semaphore_signal(barrier, inc=1, device_id={"tp": lax.rem(tp + k, n_tp)})
+
+    pairs = (
+        (tokens_hbm, tokens),
+        (gain_hbm, gain),
+        (gate_hbm.at[:, pl.ds(pl.multiple_of(me * depth, depth), depth)], gate_w),
+        (query_hbm, query_w),
+        (key_hbm, key_w),
+        (value_hbm, value_w),
+        (bias_hbm, bias),
+        (parents_hbm, parents),
+        (lengths_hbm, lengths),
+        (decay_hbm, decay),
+        (out_hbm, out_w),
+    )
+    loads = [pltpu.make_async_copy(src, dst, load_sem.at[i]) for i, (src, dst) in enumerate(pairs)]
+    for load in loads:
+        load.start()
+    for s in range(seqs):
+        pltpu.make_async_copy(keys_hbm.at[s], keys.at[s], cache_sem.at[0, s]).start()
+        pltpu.make_async_copy(values_hbm.at[s], values.at[s], cache_sem.at[1, s]).start()
+    load_of = dict(
+        zip(("tokens", "gain", "gate", "q", "k", "v", "bias", "parents", "lengths", "decay", "out"), loads)
+    )
+
+    def iota(shape, dim):
+        return lax.broadcasted_iota(jnp.int32, shape, dim)
+
+    def far_id(d):
+        return lax.rem(far + d, n_far)
+
+    def near_id(z, x):
+        return {"kv": z * 2 + x}
+
+    own_half = pl.multiple_of(side * half, half)
+    peer_half = pl.multiple_of((1 - side) * half, half)
+
+    load_of["tokens"].wait()
+    load_of["gain"].wait()
+    xf = tokens[...].astype(F32)
+    feats[:, :depth] = (xf * gain[...]).astype(BF16)
+    square = xf * xf
+    high = square.astype(BF16)
+    feats[:, depth : 2 * depth] = high
+    feats[:, 2 * depth :] = (square - high.astype(F32)).astype(BF16)
+
+    load_of["gate"].wait()
+    t_rows = n_far * 8
+    p_row = iota((t_rows, gate_w.shape[0]), 0)
+    p_col = iota((t_rows, gate_w.shape[0]), 1)
+    p_in = lax.rem(p_row, 8)
+    wanted = (p_in < own_heads) & (p_col == tp * heads + lax.div(p_row, 8) * own_heads + p_in)
+    gates = dot(wanted.astype(BF16), gate_w[...]).astype(BF16)
+    ones = (lax.rem(iota((t_rows, depth), 0), 8) == own_heads).astype(BF16)
+    tails = jnp.concatenate([gates, ones, ones], axis=1)
+
+    def project_q(base, dst):
+        full = dot(feats[pl.ds(base, half), :depth], query_w[...])
+        for i in range(waves):
+            piece = full[i * wrows : (i + 1) * wrows]
+            tail = dot_nt(tails, feats[pl.ds(base + i * wrows, wrows), :])
+            tail = jnp.concatenate([tail, jnp.zeros((t_rows, LANES - wrows), F32)], axis=1)
+            for f in range(n_far):
+                dst[i, f, :wrows] = piece[:, f * cols : (f + 1) * cols]
+                dst[i, f, wrows:] = tail[f * 8 : (f + 1) * 8]
+
+    def project_kv(base, dst):
+        for which, w in enumerate((key_w, value_w)):
+            full = dot(feats[pl.ds(base, half), :depth], w[...])
+            for i in range(waves):
+                piece = full[i * wrows : (i + 1) * wrows].astype(dst.dtype)
+                for f in range(n_far):
+                    dst[i, f, which * wrows : (which + 1) * wrows] = piece[:, f * cols : (f + 1) * cols]
+
+    def x_copy(i, src, dst, send, recv):
+        return pltpu.make_async_remote_copy(
+            src_ref=src.at[i],
+            dst_ref=dst.at[i],
+            send_sem=send.at[i],
+            recv_sem=recv.at[i],
+            device_id=near_id(far, 1 - side),
+        )
+
+    def z_copy(i, d, src, dst, send, recv):
+        return pltpu.make_async_remote_copy(
+            src_ref=src.at[i, far_id(d)],
+            dst_ref=dst.at[d - 1, i],
+            send_sem=send.at[d - 1, i],
+            recv_sem=recv.at[d - 1, i],
+            device_id=near_id(far_id(d), side),
+        )
+
+    load_of["q"].wait()
+    project_q(peer_half, q_out)
+    pl.semaphore_wait(barrier, n + n_tp - 2)
+    for i in range(waves):
+        x_copy(i, q_out, q_in, qx_send, qx_recv).start()
+    load_of["k"].wait()
+    load_of["v"].wait()
+    project_kv(peer_half, kv_out)
+    for i in range(waves):
+        x_copy(i, kv_out, kv_in, kx_send, kx_recv).start()
+    project_q(own_half, q_own)
+    project_kv(own_half, kv_own)
+
+    load_of["bias"].wait()
+    load_of["parents"].wait()
+    load_of["lengths"].wait()
+    load_of["decay"].wait()
+    par_pad[...] = jnp.zeros(par_pad.shape, jnp.int32)
+    par_pad[0:seqs, 0:props] = parents[...]
+    r_i = iota((LANES, LANES), 0)
+    c_i = iota((LANES, LANES), 1)
+    lane1 = iota((1, LANES), 1)
+    eye = r_i == c_i
+    for i in range(waves):
+        row = jnp.full((1, LANES), -1, jnp.int32)
+        for j in range(wave):
+            of = par_pad[pl.ds(side * half_seqs + i * wave + j, 1), :]
+            if j:
+                of = pltpu.roll(jnp.broadcast_to(of, (8, LANES)), j * props, 1)[0:1]
+            inside = (lane1 >= j * props) & (lane1 < (j + 1) * props)
+            row = jnp.where(inside, of + j * props, row)
+        link = ((row == r_i) | eye).astype(F32).astype(BF16)
+        for _ in range(props.bit_length()):
+            link = jnp.minimum(dot(link, link), 1.0).astype(BF16)
+        link_s[i] = link
+        anc_s[i] = dot_nt(eye.astype(F32).astype(BF16), link)
+    w_row = lax.rem(iota(widen.shape, 0), LANES)
+    w_col = iota(widen.shape, 1)
+    w_src = lax.div(w_col, cols) * 8 + lax.div(lax.rem(w_col, cols), head_dim)
+    widen[...] = (w_row == w_src).astype(F32).astype(BF16)
+    b_shape = (8, bias.shape[1])
+    b_row, b_col = iota(b_shape, 0), iota(b_shape, 1)
+    mine = (b_row < own_heads) & (b_col == tp * heads + far * own_heads + b_row)
+    bias_col = jnp.sum(jnp.where(mine, jnp.broadcast_to(bias[...], b_shape), 0.0), axis=1, keepdims=True)
+
+    for i in range(waves):
+        x_copy(i, q_out, q_in, qx_send, qx_recv).wait_recv()
+        q_own[i] = q_own[i] + q_in[i]
+        for d in range(1, n_far):
+            z_copy(i, d, q_own, q_far, qz_send, qz_recv).start()
+
+    targets = [(d, 0) for d in range(1, n_far)] + [(d, 1) for d in range(n_far)]
+
+    def target_id(d, cross):
+        return near_id(far_id(d), side if not cross else 1 - side)
+
+    def spread_copy(i, t, buf, send, recv):
+        d, cross = targets[t]
+        block = side * waves + i
+        return pltpu.make_async_remote_copy(
+            src_ref=buf.at[block, far],
+            dst_ref=buf.at[block, far],
+            send_sem=send.at[t, i],
+            recv_sem=recv.at[block, far],
+            device_id=target_id(d, cross),
+        )
+
+    def spread_wait(i, t, buf, send, recv):
+        d, cross = targets[t]
+        block = (1 - side if cross else side) * waves + i
+        pltpu.make_async_remote_copy(
+            src_ref=buf.at[block, far_id(d)],
+            dst_ref=buf.at[block, far_id(d)],
+            send_sem=send.at[t, i],
+            recv_sem=recv.at[block, far_id(d)],
+            device_id=target_id(d, cross),
+        ).wait_recv()
+
+    lane8 = iota((8, LANES), 1)
+    row8 = iota((8, LANES), 0)
+
+    def owner_q(i):
+        total = q_own[i, far]
+        for d in range(1, n_far):
+            z_copy(i, d, q_own, q_far, qz_send, qz_recv).wait_recv()
+            total = total + q_far[d - 1, i]
+        tail = total[wrows:]
+        inverse = lax.rsqrt(tail / (depth * n) + 1e-06)
+        column = tile_rows(inverse, LANES).T[:wrows, own_heads : own_heads + 1]
+        inv_s[i] = jnp.broadcast_to(column, (wrows, cols))
+        qbuf[side * waves + i, far] = (inv_s[i] * total[:wrows]).astype(BF16)
+        for t in range(sources):
+            spread_copy(i, t, qbuf, b_send, b_recv).start()
+        inverse_row = jnp.broadcast_to(inverse[own_heads : own_heads + 1], (8, LANES))
+        x = inverse_row * tail + bias_col
+        log_gate = jnp.minimum(x, 0.0) - jnp.log1p(jnp.exp(-jnp.abs(x)))
+        log_gate = jnp.where((row8 < own_heads) & (lane8 < wrows), log_gate, 0.0)
+        parts = dot(jnp.concatenate(split3(log_gate), axis=0), link_s[i])
+        path_s[i] = parts[:8] + parts[8:16] + parts[16:24]
+
+    for i in range(waves):
+        owner_q(i)
+
+    for i in range(waves):
+        x_copy(i, kv_out, kv_in, kx_send, kx_recv).wait_recv()
+        kv_own[i] = kv_own[i] + kv_in[i].astype(F32)
+        kv_pass[i] = kv_own[i].astype(BF16)
+        for d in range(1, n_far):
+            z_copy(i, d, kv_pass, kv_far, kz_send, kz_recv).start()
+
+    group = min(heads, 256 // head_dim)
+    gwidth = group * head_dim
+    g_head = iota((group, props, gwidth), 0)
+    g_col = lax.div(iota((group, props, gwidth), 2), head_dim)
+    g_diag = (g_head == g_col).reshape(group * props, gwidth)
+    lane_w = iota((wrows, LANES), 1)
+    position = iota((heads, pos_dev), 1) + me * pos_dev
+
+    def mix_copy(i, t, which, src, dst):
+        d, cross = targets[t]
+        block = (1 - side if cross else side) * waves + i
+        return pltpu.make_async_remote_copy(
+            src_ref=src.at[block, far_id(d)],
+            dst_ref=dst.at[t, i],
+            send_sem=c_send.at[which, t, i],
+            recv_sem=c_recv.at[which, t, i],
+            device_id=target_id(d, cross),
+        )
+
+    def attend(i, cross):
+        place = 1 - side if cross else side
+        block = place * waves + i
+        for t in range(sources):
+            if targets[t][1] == cross:
+                spread_wait(i, t, qbuf, b_send, b_recv)
+        q_wave = jnp.concatenate([qbuf[block, f] for f in range(n_far)], axis=1).astype(F32)
+        if exact_scale:
+            q_wave = q_wave * scale
+        mixes, tops, totals = [], [], []
+        for j in range(wave):
+            s = place * half_seqs + i * wave + j
+            pltpu.make_async_copy(keys_hbm.at[s], keys.at[s], cache_sem.at[0, s]).wait()
+            pltpu.make_async_copy(values_hbm.at[s], values.at[s], cache_sem.at[1, s]).wait()
+            fade = jnp.where(position < lengths[s], decay[s], LOW)
+            m_parts, t_parts, n_parts = [], [], []
+            for g in range(heads // group):
+                q = q_wave[j * props : (j + 1) * props, g * gwidth : (g + 1) * gwidth]
+                q = jnp.broadcast_to(q[None], (group, props, gwidth)).reshape(group * props, gwidth)
+                q = jnp.where(g_diag, q, 0.0).astype(BF16)
+                scores = dot_nt(q, keys[s, :, g * gwidth : (g + 1) * gwidth])
+                if not exact_scale:
+                    scores = scores * scale
+                fades = [
+                    jnp.broadcast_to(fade[h : h + 1], (props, pos_dev))
+                    for h in range(g * group, (g + 1) * group)
+                ]
+                scores = scores + jnp.concatenate(fades, axis=0)
+                top = jnp.max(scores, axis=1, keepdims=True)
+                w = jnp.exp(scores - top)
+                total = jnp.sum(w, axis=1, keepdims=True)
+                m = dot(w.astype(BF16), values[s, :, g * gwidth : (g + 1) * gwidth])
+                m = jnp.where(g_diag, m, 0.0).reshape(group, props, gwidth)
+                m_parts.append(jnp.sum(m, axis=0))
+                for h in range(group):
+                    t_parts.append(top[h * props : (h + 1) * props])
+                    n_parts.append(total[h * props : (h + 1) * props])
+            mixes.append(jnp.concatenate(m_parts, axis=1))
+            tops.append(t_parts)
+            totals.append(n_parts)
+        mixed = jnp.concatenate(mixes, axis=0).astype(BF16)
+        for f in range(n_far):
+            mix[block, f] = mixed[:, f * cols : (f + 1) * cols]
+        acc = jnp.zeros((wrows, LANES), F32)
+        for h in range(heads):
+            f, k = divmod(h, own_heads)
+            for at, cols_of in ((k, tops), (own_heads + k, totals)):
+                col = jnp.concatenate([cols_of[j][h] for j in range(wave)], axis=0)
+                acc = jnp.where(lane_w == f * 8 + at, col, acc)
+        flat = tile_rows(acc, LANES).T
+        for f in range(n_far):
+            stat[block, f] = flat[f * 8 : (f + 1) * 8]
+        for t in range(sources):
+            if targets[t][1] == cross:
+                mix_copy(i, t, 0, mix, mix_in).start()
+                mix_copy(i, t, 1, stat, stat_in).start()
+
+    own_head_of = lax.div(iota((wrows, cols), 1), head_dim)
+
+    def tree(i):
+        block = side * waves + i
+        total = kv_own[i, far]
+        for d in range(1, n_far):
+            z_copy(i, d, kv_pass, kv_far, kz_send, kz_recv).wait_recv()
+            total = total + kv_far[d - 1, i].astype(F32)
+        new_k = tile_rows(inv_s[i] * total[:wrows], LANES).astype(BF16)
+        new_v = tile_rows(inv_s[i] * total[wrows:], LANES).astype(BF16)
+        q = qbuf[block, far].astype(F32)
+        q = jnp.concatenate([jnp.where(own_head_of == h, q, 0.0) for h in range(own_heads)], axis=0)
+        scores = dot_nt(q.astype(BF16), new_k) * scale
+        path = path_s[i]
+        path_cols = tile_rows(path, LANES).T[:wrows]
+        shifts = [path_cols[:, h : h + 1] - path[h : h + 1] for h in range(own_heads)]
+        scores = scores + jnp.concatenate(shifts, axis=0)
+        live = jnp.concatenate([anc_s[i, :wrows]] * own_heads, axis=0) > 0.5
+        scores = jnp.where(live, scores, LOW)
+        top = jnp.max(scores, axis=1, keepdims=True)
+        w = jnp.where(live, jnp.exp(scores - top), 0.0)
+        total = jnp.sum(w, axis=1, keepdims=True)
+        m = dot(w.astype(BF16), new_v)
+        merged = jnp.zeros((wrows, cols), F32)
+        acc = jnp.zeros((wrows, LANES), F32)
+        for h in range(own_heads):
+            part = slice(h * wrows, (h + 1) * wrows)
+            merged = jnp.where(own_head_of == h, m[part], merged)
+            acc = jnp.where(lane_w == h, top[part], acc)
+            acc = jnp.where(lane_w == own_heads + h, total[part], acc)
+        tmix[i] = merged
+        tstat[i] = tile_rows(acc, LANES).T[:8]
+
+    def merge(i):
+        block = side * waves + i
+        for t in range(sources):
+            mix_copy(i, t, 0, mix, mix_in).wait_recv()
+            mix_copy(i, t, 1, stat, stat_in).wait_recv()
+        stats = [stat[block, far]] + [stat_in[t, i] for t in range(sources)]
+        path = path_s[i]
+        tops = [st + path for st in stats] + [tstat[i]]
+        totals = [pltpu.roll(st, 8 - own_heads, 0) for st in stats + [tstat[i]]]
+        best = functools.reduce(jnp.maximum, tops)
+        factors = [jnp.exp(top - best) for top in tops]
+        denom = functools.reduce(jnp.add, [f * t for f, t in zip(factors, totals)])
+        factors = [jnp.where(row8 < own_heads, f / denom, 0.0) for f in factors]
+        turned = tile_rows(jnp.concatenate(factors, axis=0), LANES).T[:wrows]
+        high = turned.astype(BF16)
+        low = (turned - high.astype(F32)).astype(BF16)
+        wide = dot(jnp.concatenate([high, low], axis=1), widen[...])
+        mixes = [mix[block, far]] + [mix_in[t, i] for t in range(sources)] + [tmix[i]]
+        numer = jnp.zeros((wrows, cols), F32)
+        for k, m in enumerate(mixes):
+            numer = numer + wide[:, k * cols : (k + 1) * cols] * m.astype(F32)
+        att[block, far] = numer.astype(BF16)
+        for t in range(sources):
+            spread_copy(i, t, att, d_send, d_recv).start()
+
+    per_tp = seqs // n_tp
+
+    def e_copy(s, t):
+        k = jnp.maximum(lax.rem(tp - t + n_tp, n_tp) - 1, 0)
+        return pltpu.make_async_remote_copy(
+            src_ref=terms.at[s],
+            dst_ref=terms_in.at[k, lax.rem(s, per_tp)],
+            send_sem=e_send.at[s],
+            recv_sem=e_recv.at[k, lax.rem(s, per_tp)],
+            device_id={"tp": t},
+        )
+
+    def output(i, cross):
+        place = 1 - side if cross else side
+        block = place * waves + i
+        for t in range(sources):
+            if targets[t][1] == cross:
+                spread_wait(i, t, att, d_send, d_recv)
+        attended = jnp.concatenate([att[block, f] for f in range(n_far)], axis=1)
+        term = dot(attended, out_w[...])
+        for j in range(wave):
+            s = place * half_seqs + i * wave + j
+            terms[s] = fold(term[j * props : (j + 1) * props]).astype(BF16)
+            t = lax.div(s, per_tp)
+            pl.when(tp != t)(e_copy(s, t).start)
+
+    for i in range(waves):
+        for cross in range(2):
+            attend(i, cross)
+        if i > 0:
+            merge(i - 1)
+        tree(i)
+    merge(waves - 1)
+    load_of["out"].wait()
+    for i in range(waves):
+        for cross in range(2):
+            output(i, cross)
+
+    done = []
+    for j in range(per_tp):
+        total = unfold(terms[tp * per_tp + j])
+        for k in range(1, n_tp):
+            pltpu.make_async_remote_copy(
+                src_ref=terms.at[0],
+                dst_ref=terms_in.at[k - 1, j],
+                send_sem=e_send.at[0],
+                recv_sem=e_recv.at[k - 1, j],
+                device_id={"tp": lax.rem(tp + k, n_tp)},
+            ).wait_recv()
+            total = total + unfold(terms_in[k - 1, j])
+        done.append(total)
+    out[...] = jnp.concatenate(done, axis=0).astype(BF16)
+
+    for i in range(waves):
+        x_copy(i, q_out, q_in, qx_send, qx_recv).wait_send()
+        x_copy(i, kv_out, kv_in, kx_send, kx_recv).wait_send()
+        for d in range(1, n_far):
+            z_copy(i, d, q_own, q_far, qz_send, qz_recv).wait_send()
+            z_copy(i, d, kv_pass, kv_far, kz_send, kz_recv).wait_send()
+        for t in range(sources):
+            spread_copy(i, t, qbuf, b_send, b_recv).wait_send()
+            spread_copy(i, t, att, d_send, d_recv).wait_send()
+            mix_copy(i, t, 0, mix, mix_in).wait_send()
+            mix_copy(i, t, 1, stat, stat_in).wait_send()
+    for s in range(seqs):
+        t = s // per_tp
+        pl.when(tp != t)(e_copy(s, t).wait_send)
+
+
+def wave_size(n, n_tp, seqs, props, heads, width):
+    n_far = n // 2
+    if n % 2 or seqs % 2 or seqs % n_tp or heads % n_far or width % (n_far * LANES):
+        return 0
+    head_dim = width // heads
+    own = heads // n_far
+    if own > 4 or 8 * (n + 1) > LANES or (heads % min(heads, max(256 // head_dim, 1))):
+        return 0
+    for wave in range(1, seqs // 2 + 1):
+        fits = wave * props % 16 == 0 and wave * props <= LANES
+        if seqs // 2 % wave == 0 and fits and props % 8 == 0:
+            return wave
+    return 0
+
+
 def solution(mesh):
     n, n_tp = mesh.shape["kv"], mesh.shape["tp"]
 
@@ -534,12 +1068,78 @@
         vmem = pl.BlockSpec(memory_space=pltpu.VMEM)
         hbm = pl.BlockSpec(memory_space=pltpu.HBM)
         dma = pltpu.SemaphoreType.DMA
-        return pl.pallas_call(
-            functools.partial(kernel, n, n_tp),
-            out_shape=jax.ShapeDtypeStruct((block, cols), BF16),
-            in_specs=[hbm] * 13,
-            out_specs=vmem,
-            scratch_shapes=[
+        wave = wave_size(n, n_tp, seqs, props, heads, width)
+        if wave:
+            n_far = n // 2
+            waves = seqs // 2 // wave
+            wrows = wave * props
+            wcols = width // n_far
+            per_tp = seqs // n_tp
+            block_q = (n_far, wrows + 8, wcols)
+            block_kv = (n_far, 2 * wrows, wcols)
+            body_of = functools.partial(by_heads, n, n_tp, wave)
+            scratch = [
+                pltpu.VMEM(tokens.shape, BF16),
+                pltpu.VMEM((1, depth), F32),
+                pltpu.VMEM(query_weight.shape, BF16),
+                pltpu.VMEM(key_weight.shape, BF16),
+                pltpu.VMEM(value_weight.shape, BF16),
+                pltpu.VMEM((gate_weight.shape[1], depth), BF16),
+                pltpu.VMEM((1, gate_bias.shape[0]), F32),
+                pltpu.VMEM(cache_decay.shape, F32),
+                pltpu.SMEM(lengths.shape, jnp.int32),
+                pltpu.VMEM(parents.shape, jnp.int32),
+                pltpu.VMEM(out_weight.shape, BF16),
+                pltpu.VMEM(cache_keys.shape, BF16),
+                pltpu.VMEM(cache_values.shape, BF16),
+                pltpu.VMEM((rows, 3 * depth), BF16),
+                pltpu.VMEM((waves,) + block_q, F32),
+                pltpu.VMEM((waves,) + block_q, F32),
+                pltpu.VMEM((waves,) + block_q, F32),
+                pltpu.VMEM((n_far - 1, waves) + block_q[1:], F32),
+                pltpu.VMEM((waves,) + block_kv, BF16),
+                pltpu.VMEM((waves,) + block_kv, BF16),
+                pltpu.VMEM((waves,) + block_kv, F32),
+                pltpu.VMEM((waves,) + block_kv, BF16),
+                pltpu.VMEM((n_far - 1, waves) + block_kv[1:], BF16),
+                pltpu.VMEM((2 * waves, n_far, wrows, wcols), BF16),
+                pltpu.VMEM((2 * waves, n_far, wrows, wcols), BF16),
+                pltpu.VMEM((n - 1, waves, wrows, wcols), BF16),
+                pltpu.VMEM((2 * waves, n_far, 8, LANES), F32),
+                pltpu.VMEM((n - 1, waves, 8, LANES), F32),
+                pltpu.VMEM((2 * waves, n_far, wrows, wcols), BF16),
+                pltpu.VMEM((seqs,) + folded, BF16),
+                pltpu.VMEM((n_tp - 1, per_tp) + folded, BF16),
+                pltpu.VMEM((-(-seqs // 8) * 8, LANES), jnp.int32),
+                pltpu.VMEM((waves, LANES, LANES), BF16),
+                pltpu.VMEM((waves, LANES, LANES), F32),
+                pltpu.VMEM((waves, 8, LANES), F32),
+                pltpu.VMEM((waves, wrows, wcols), F32),
+                pltpu.VMEM((waves, wrows, wcols), F32),
+                pltpu.VMEM((waves, 8, LANES), F32),
+                pltpu.VMEM((2 * LANES, (n + 1) * wcols), BF16),
+                dma((11,)),
+                dma((2, seqs)),
+                dma((waves,)),
+                dma((waves,)),
+                dma((waves,)),
+                dma((waves,)),
+                dma((n_far - 1, waves)),
+                dma((n_far - 1, waves)),
+                dma((n_far - 1, waves)),
+                dma((n_far - 1, waves)),
+                dma((n - 1, waves)),
+                dma((2 * waves, n_far)),
+                dma((2, n - 1, waves)),
+                dma((2, n - 1, waves)),
+                dma((n - 1, waves)),
+                dma((2 * waves, n_far)),
+                dma((seqs,)),
+                dma((n_tp - 1, per_tp)),
+            ]
+        else:
+            body_of = functools.partial(by_sequence, n, n_tp)
+            scratch = [
                 pltpu.VMEM(tokens.shape, BF16),
                 pltpu.VMEM((1, depth), F32),
                 pltpu.VMEM(query_weight.shape, BF16),
@@ -588,7 +1188,13 @@
                 dma((seqs,)),
                 dma((n_tp,)),
                 dma((n_tp - 1,)),
-            ],
+            ]
+        return pl.pallas_call(
+            body_of,
+            out_shape=jax.ShapeDtypeStruct((block, cols), BF16),
+            in_specs=[hbm] * 13,
+            out_specs=vmem,
+            scratch_shapes=scratch,
             compiler_params=pltpu.CompilerParams(
                 collective_id=0, has_side_effects=True, vmem_limit_bytes=67_043_328
             ),

time: 70.1 us -> 57.6 us (0.82)
  Pallas kernels: 68.4 us -> 55.8 us
    pallas_call x1, Pallas kernels: 68.4 us -> 55.8 us  [body(): pl.pallas_call(body_of, out_shape=jax.ShapeDtypeStruct((block, cols), BF1...]
where the time goes in v2:
time: 57.6 us; the launch traced here: 57.3 us
  Pallas kernels  55.8 us (97%)
  local copies, waits for them, and re-layouts  1.52 us (3%)
    pallas_call x1, Pallas kernels, body(): pl.pallas_call(body_of, out_shape=jax.ShapeDtypeStruct((block, cols), BF1...  55.8 us
    unnamed x1, local copies, waits for them, and re-layouts  1.52 us

profile of v2, /device:TPU:0, one launch (start us, length us, event | category | flops | bytes accessed | tf_op | source)
XLA Modules:
  0.0 57.3 jit_solution(17613561367519781751)
XLA Ops:
  0.0 55.8 %shard_map.127 = bf16[72,512]{1,0:T(8,128)(2,1)} custom-call(bf16[288,512]{1,0:T(8,128)(2,1)} %tokens_hbm.1, f32[1,512]{1,0:T(1,128)} %bitcast.4, bf16[512,512]{1,0:T(8,128)(2,1)} %query_hbm.1, bf16[512,512]{1,0:T(8,128)(2,1)} %key_hbm.1, bf16[512,512]{1,0:T(8,128)(2,1)} %value_hbm.1, bf16[32,4096]{1,0:T(8,128)(2,1)} %bitcast.3, f32[1,32]{1,0:T(1,128)} %bitcast.5, ...), custom_call_target="tpu_custom_call" | custom-call | tf_op jit(solution)/shard_map/pallas_call | solution.py:1192
  55.8 1.5 %copy.15 = bf16[72,512]{1,0:T(8,128)(2,1)} copy(bf16[72,512]{1,0:T(8,128)(2,1)} %shard_map.127) | data formatting | bytes 147456

commit v3 on v2

--- a/solution.py
+++ b/solution.py
@@ -552,6 +552,9 @@
     q_in,
     q_own,
     q_far,
+    q_last,
+    q_last_in,
+    q_cross,
     kv_out,
     kv_in,
     kv_own,
@@ -591,6 +594,12 @@
     d_recv,
     e_send,
     e_recv,
+    qr_send,
+    qr_recv,
+    ar_send,
+    ar_recv,
+    l_send,
+    l_recv,
 ):
     me = lax.axis_index("kv")
     tp = lax.axis_index("tp")
@@ -613,12 +622,6 @@
     wrows = wave * props
     sources = n - 1
 
-    barrier = pltpu.get_barrier_semaphore()
-    for k in range(1, n):
-        pl.semaphore_signal(barrier, inc=1, device_id={"kv": lax.rem(me + k, n)})
-    for k in range(1, n_tp):
-        pl.semaphore_signal(barrier, inc=1, device_id={"tp": lax.rem(tp + k, n_tp)})
-
     pairs = (
         (tokens_hbm, tokens),
         (gain_hbm, gain),
@@ -633,29 +636,36 @@
         (out_hbm, out_w),
     )
     loads = [pltpu.make_async_copy(src, dst, load_sem.at[i]) for i, (src, dst) in enumerate(pairs)]
-    for load in loads:
+    load_of = dict(
+        zip(("tokens", "gain", "gate", "q", "k", "v", "bias", "parents", "lengths", "decay", "out"), loads)
+    )
+    for load in loads[:6]:
+        load.start()
+    barrier = pltpu.get_barrier_semaphore()
+    for k in range(1, n):
+        pl.semaphore_signal(barrier, inc=1, device_id={"kv": lax.rem(me + k, n)})
+    for k in range(1, n_tp):
+        pl.semaphore_signal(barrier, inc=1, device_id={"tp": lax.rem(tp + k, n_tp)})
+
+    def iota(shape, dim):
+        return lax.broadcasted_iota(jnp.int32, shape, dim)
+
+    def far_id(d):
+        return lax.rem(far + d, n_far)
+
+    def near_id(z, x):
+        return {"kv": z * 2 + x}
+
+    own_half = pl.multiple_of(side * half, half)
+    peer_half = pl.multiple_of((1 - side) * half, half)
+
+    load_of["tokens"].wait()
+    load_of["gain"].wait()
+    for load in loads[6:]:
         load.start()
     for s in range(seqs):
         pltpu.make_async_copy(keys_hbm.at[s], keys.at[s], cache_sem.at[0, s]).start()
         pltpu.make_async_copy(values_hbm.at[s], values.at[s], cache_sem.at[1, s]).start()
-    load_of = dict(
-        zip(("tokens", "gain", "gate", "q", "k", "v", "bias", "parents", "lengths", "decay", "out"), loads)
-    )
-
-    def iota(shape, dim):
-        return lax.broadcasted_iota(jnp.int32, shape, dim)
-
-    def far_id(d):
-        return lax.rem(far + d, n_far)
-
-    def near_id(z, x):
-        return {"kv": z * 2 + x}
-
-    own_half = pl.multiple_of(side * half, half)
-    peer_half = pl.multiple_of((1 - side) * half, half)
-
-    load_of["tokens"].wait()
-    load_of["gain"].wait()
     xf = tokens[...].astype(F32)
     feats[:, :depth] = (xf * gain[...]).astype(BF16)
     square = xf * xf
@@ -673,15 +683,21 @@
     ones = (lax.rem(iota((t_rows, depth), 0), 8) == own_heads).astype(BF16)
     tails = jnp.concatenate([gates, ones, ones], axis=1)
 
-    def project_q(base, dst):
+    def project_q(base, dst, which):
         full = dot(feats[pl.ds(base, half), :depth], query_w[...])
         for i in range(waves):
             piece = full[i * wrows : (i + 1) * wrows]
             tail = dot_nt(tails, feats[pl.ds(base + i * wrows, wrows), :])
             tail = jnp.concatenate([tail, jnp.zeros((t_rows, LANES - wrows), F32)], axis=1)
             for f in range(n_far):
-                dst[i, f, :wrows] = piece[:, f * cols : (f + 1) * cols]
-                dst[i, f, wrows:] = tail[f * 8 : (f + 1) * 8]
+                for at, rows_of in (
+                    (slice(0, wrows), piece[:, f * cols : (f + 1) * cols]),
+                    (slice(wrows, wrows + 8), tail[f * 8 : (f + 1) * 8]),
+                ):
+                    if i < waves - 1:
+                        dst[i, f, at] = rows_of
+                    else:
+                        q_last[f, which, at] = rows_of
 
     def project_kv(base, dst):
         for which, w in enumerate((key_w, value_w)):
@@ -709,17 +725,37 @@
             device_id=near_id(far_id(d), side),
         )
 
+    def last_copy(d):
+        return pltpu.make_async_remote_copy(
+            src_ref=q_last.at[far_id(d)],
+            dst_ref=q_last_in.at[d - 1],
+            send_sem=l_send.at[d - 1],
+            recv_sem=l_recv.at[d - 1],
+            device_id=near_id(far_id(d), side),
+        )
+
+    def last_cross():
+        return pltpu.make_async_remote_copy(
+            src_ref=q_last.at[far, 1],
+            dst_ref=q_cross,
+            send_sem=l_send.at[n_far - 1],
+            recv_sem=l_recv.at[n_far - 1],
+            device_id=near_id(far, 1 - side),
+        )
+
     load_of["q"].wait()
-    project_q(peer_half, q_out)
+    project_q(peer_half, q_out, 1)
     pl.semaphore_wait(barrier, n + n_tp - 2)
-    for i in range(waves):
+    for i in range(waves - 1):
         x_copy(i, q_out, q_in, qx_send, qx_recv).start()
+    project_q(own_half, q_own, 0)
+    for d in range(1, n_far):
+        last_copy(d).start()
     load_of["k"].wait()
     load_of["v"].wait()
     project_kv(peer_half, kv_out)
     for i in range(waves):
         x_copy(i, kv_out, kv_in, kx_send, kx_recv).start()
-    project_q(own_half, q_own)
     project_kv(own_half, kv_own)
 
     load_of["bias"].wait()
@@ -754,11 +790,15 @@
     mine = (b_row < own_heads) & (b_col == tp * heads + far * own_heads + b_row)
     bias_col = jnp.sum(jnp.where(mine, jnp.broadcast_to(bias[...], b_shape), 0.0), axis=1, keepdims=True)
 
-    for i in range(waves):
+    for i in range(waves - 1):
         x_copy(i, q_out, q_in, qx_send, qx_recv).wait_recv()
         q_own[i] = q_own[i] + q_in[i]
         for d in range(1, n_far):
             z_copy(i, d, q_own, q_far, qz_send, qz_recv).start()
+    for d in range(1, n_far):
+        last_copy(d).wait_recv()
+    q_last[far] = q_last[far] + functools.reduce(jnp.add, [q_last_in[d] for d in range(n_far - 1)])
+    last_cross().start()
 
     targets = [(d, 0) for d in range(1, n_far)] + [(d, 1) for d in range(n_far)]
 
@@ -775,6 +815,26 @@
             recv_sem=recv.at[block, far],
             device_id=target_id(d, cross),
         )
+
+    def relay_copy(i, buf, send, recv):
+        block = side * waves + i
+        return pltpu.make_async_remote_copy(
+            src_ref=buf.at[block],
+            dst_ref=buf.at[block],
+            send_sem=send.at[i],
+            recv_sem=recv.at[i],
+            device_id=near_id(far, 1 - side),
+        )
+
+    def spread(i, direct, buf, send, recv):
+        for t in range(sources if direct else n_far - 1):
+            spread_copy(i, t, buf, send, recv).start()
+
+    def sent(i, direct, buf, send, recv, r_send, r_recv):
+        for t in range(sources if direct else n_far - 1):
+            spread_copy(i, t, buf, send, recv).wait_send()
+        if not direct:
+            relay_copy(i, buf, r_send, r_recv).wait_send()
 
     def spread_wait(i, t, buf, send, recv):
         d, cross = targets[t]
@@ -787,21 +847,42 @@
             device_id=target_id(d, cross),
         ).wait_recv()
 
+    def pass_on(i, direct, buf, send, recv, r_send, r_recv):
+        for t in range(n_far - 1):
+            spread_wait(i, t, buf, send, recv)
+        if not direct:
+            relay_copy(i, buf, r_send, r_recv).start()
+
+    def crossed(i, direct, buf, send, recv, r_send, r_recv):
+        if not direct:
+            relay_copy(i, buf, r_send, r_recv).wait_recv()
+            return
+        for t in range(n_far - 1, sources):
+            spread_wait(i, t, buf, send, recv)
+
+    q_route = (qbuf, b_send, b_recv, qr_send, qr_recv)
+    a_route = (att, d_send, d_recv, ar_send, ar_recv)
+    q_direct = [False] * waves
+    a_direct = [i > 0 for i in range(waves)]
+
     lane8 = iota((8, LANES), 1)
     row8 = iota((8, LANES), 0)
 
     def owner_q(i):
-        total = q_own[i, far]
-        for d in range(1, n_far):
-            z_copy(i, d, q_own, q_far, qz_send, qz_recv).wait_recv()
-            total = total + q_far[d - 1, i]
+        if i < waves - 1:
+            total = q_own[i, far]
+            for d in range(1, n_far):
+                z_copy(i, d, q_own, q_far, qz_send, qz_recv).wait_recv()
+                total = total + q_far[d - 1, i]
+        else:
+            last_cross().wait_recv()
+            total = q_last[far, 0] + q_cross[...]
         tail = total[wrows:]
         inverse = lax.rsqrt(tail / (depth * n) + 1e-06)
         column = tile_rows(inverse, LANES).T[:wrows, own_heads : own_heads + 1]
         inv_s[i] = jnp.broadcast_to(column, (wrows, cols))
         qbuf[side * waves + i, far] = (inv_s[i] * total[:wrows]).astype(BF16)
-        for t in range(sources):
-            spread_copy(i, t, qbuf, b_send, b_recv).start()
+        spread(i, q_direct[i], qbuf, b_send, b_recv)
         inverse_row = jnp.broadcast_to(inverse[own_heads : own_heads + 1], (8, LANES))
         x = inverse_row * tail + bias_col
         log_gate = jnp.minimum(x, 0.0) - jnp.log1p(jnp.exp(-jnp.abs(x)))
@@ -812,12 +893,41 @@
     for i in range(waves):
         owner_q(i)
 
-    for i in range(waves):
-        x_copy(i, kv_out, kv_in, kx_send, kx_recv).wait_recv()
-        kv_own[i] = kv_own[i] + kv_in[i].astype(F32)
-        kv_pass[i] = kv_own[i].astype(BF16)
-        for d in range(1, n_far):
-            z_copy(i, d, kv_pass, kv_far, kz_send, kz_recv).start()
+    strides = [1 << b for b in range(n_far.bit_length() - 1)]
+
+    def halve_copy(i, st, m):
+        slot = sum(n_far // (2 * x) for x in strides if x < st) + m
+        partner = far + st - 2 * st * lax.rem(lax.div(far, st), 2)
+        return pltpu.make_async_remote_copy(
+            src_ref=kv_pass.at[i, lax.rem(partner, 2 * st) + 2 * st * m],
+            dst_ref=kv_far.at[slot, i],
+            send_sem=kz_send.at[slot, i],
+            recv_sem=kz_recv.at[slot, i],
+            device_id=near_id(partner, side),
+        )
+
+    def halve_start(i, st):
+        partner = far + st - 2 * st * lax.rem(lax.div(far, st), 2)
+        for m in range(n_far // (2 * st)):
+            f = lax.rem(partner, 2 * st) + 2 * st * m
+            kv_pass[i, f] = kv_own[i, f].astype(BF16)
+            halve_copy(i, st, m).start()
+
+    def halve_wait(i, st):
+        for m in range(n_far // (2 * st)):
+            halve_copy(i, st, m).wait_recv()
+            f = lax.rem(far, 2 * st) + 2 * st * m
+            slot = sum(n_far // (2 * x) for x in strides if x < st) + m
+            kv_own[i, f] = kv_own[i, f] + kv_far[slot, i].astype(F32)
+
+    def pass_kv(i, step):
+        if step:
+            halve_wait(i, strides[step - 1])
+        else:
+            x_copy(i, kv_out, kv_in, kx_send, kx_recv).wait_recv()
+            kv_own[i] = kv_own[i] + kv_in[i].astype(F32)
+        if step < len(strides):
+            halve_start(i, strides[step])
 
     group = min(heads, 256 // head_dim)
     gwidth = group * head_dim
@@ -841,19 +951,21 @@
     def attend(i, cross):
         place = 1 - side if cross else side
         block = place * waves + i
-        for t in range(sources):
-            if targets[t][1] == cross:
-                spread_wait(i, t, qbuf, b_send, b_recv)
+        if cross:
+            crossed(i, q_direct[i], *q_route)
+        first = place * half_seqs + i * wave
+        for j in range(wave):
+            s = first + j
+            pltpu.make_async_copy(keys_hbm.at[s], keys.at[s], cache_sem.at[0, s]).wait()
+            pltpu.make_async_copy(values_hbm.at[s], values.at[s], cache_sem.at[1, s]).wait()
         q_wave = jnp.concatenate([qbuf[block, f] for f in range(n_far)], axis=1).astype(F32)
         if exact_scale:
             q_wave = q_wave * scale
-        mixes, tops, totals = [], [], []
+        chains = [(j, g) for j in range(wave) for g in range(heads // group)]
+        scores_of, w_of, tops, totals, parts = {}, {}, {}, {}, {}
         for j in range(wave):
-            s = place * half_seqs + i * wave + j
-            pltpu.make_async_copy(keys_hbm.at[s], keys.at[s], cache_sem.at[0, s]).wait()
-            pltpu.make_async_copy(values_hbm.at[s], values.at[s], cache_sem.at[1, s]).wait()
+            s = first + j
             fade = jnp.where(position < lengths[s], decay[s], LOW)
-            m_parts, t_parts, n_parts = [], [], []
             for g in range(heads // group):
                 q = q_wave[j * props : (j + 1) * props, g * gwidth : (g + 1) * gwidth]
                 q = jnp.broadcast_to(q[None], (group, props, gwidth)).reshape(group * props, gwidth)
@@ -865,19 +977,22 @@
                     jnp.broadcast_to(fade[h : h + 1], (props, pos_dev))
                     for h in range(g * group, (g + 1) * group)
                 ]
-                scores = scores + jnp.concatenate(fades, axis=0)
-                top = jnp.max(scores, axis=1, keepdims=True)
-                w = jnp.exp(scores - top)
-                total = jnp.sum(w, axis=1, keepdims=True)
-                m = dot(w.astype(BF16), values[s, :, g * gwidth : (g + 1) * gwidth])
-                m = jnp.where(g_diag, m, 0.0).reshape(group, props, gwidth)
-                m_parts.append(jnp.sum(m, axis=0))
-                for h in range(group):
-                    t_parts.append(top[h * props : (h + 1) * props])
-                    n_parts.append(total[h * props : (h + 1) * props])
-            mixes.append(jnp.concatenate(m_parts, axis=1))
-            tops.append(t_parts)
-            totals.append(n_parts)
+                scores_of[j, g] = scores + jnp.concatenate(fades, axis=0)
+        for j, g in chains:
+            top = jnp.max(scores_of[j, g], axis=1, keepdims=True)
+            w = jnp.exp(scores_of[j, g] - top)
+            total = jnp.sum(w, axis=1, keepdims=True)
+            w_of[j, g] = w.astype(BF16)
+            for h in range(group):
+                tops[j, g * group + h] = top[h * props : (h + 1) * props]
+                totals[j, g * group + h] = total[h * props : (h + 1) * props]
+        for j, g in chains:
+            m = dot(w_of[j, g], values[first + j, :, g * gwidth : (g + 1) * gwidth])
+            m = jnp.where(g_diag, m, 0.0).reshape(group, props, gwidth)
+            parts[j, g] = jnp.sum(m, axis=0)
+        mixes = [
+            jnp.concatenate([parts[j, g] for g in range(heads // group)], axis=1) for j in range(wave)
+        ]
         mixed = jnp.concatenate(mixes, axis=0).astype(BF16)
         for f in range(n_far):
             mix[block, f] = mixed[:, f * cols : (f + 1) * cols]
@@ -885,11 +1000,11 @@
         for h in range(heads):
             f, k = divmod(h, own_heads)
             for at, cols_of in ((k, tops), (own_heads + k, totals)):
-                col = jnp.concatenate([cols_of[j][h] for j in range(wave)], axis=0)
+                col = jnp.concatenate([cols_of[j, h] for j in range(wave)], axis=0)
                 acc = jnp.where(lane_w == f * 8 + at, col, acc)
         flat = tile_rows(acc, LANES).T
         for f in range(n_far):
-            stat[block, f] = flat[f * 8 : (f + 1) * 8]
+            stat[block, f] = flat[f * 8 : f * 8 + stat.shape[2]]
         for t in range(sources):
             if targets[t][1] == cross:
                 mix_copy(i, t, 0, mix, mix_in).start()
@@ -899,10 +1014,8 @@
 
     def tree(i):
         block = side * waves + i
+        pass_kv(i, len(strides))
         total = kv_own[i, far]
-        for d in range(1, n_far):
-            z_copy(i, d, kv_pass, kv_far, kz_send, kz_recv).wait_recv()
-            total = total + kv_far[d - 1, i].astype(F32)
         new_k = tile_rows(inv_s[i] * total[:wrows], LANES).astype(BF16)
         new_v = tile_rows(inv_s[i] * total[wrows:], LANES).astype(BF16)
         q = qbuf[block, far].astype(F32)
@@ -934,6 +1047,7 @@
             mix_copy(i, t, 0, mix, mix_in).wait_recv()
             mix_copy(i, t, 1, stat, stat_in).wait_recv()
         stats = [stat[block, far]] + [stat_in[t, i] for t in range(sources)]
+        stats = [tile_rows(st, 8) for st in stats]
         path = path_s[i]
         tops = [st + path for st in stats] + [tstat[i]]
         totals = [pltpu.roll(st, 8 - own_heads, 0) for st in stats + [tstat[i]]]
@@ -950,8 +1064,7 @@
         for k, m in enumerate(mixes):
             numer = numer + wide[:, k * cols : (k + 1) * cols] * m.astype(F32)
         att[block, far] = numer.astype(BF16)
-        for t in range(sources):
-            spread_copy(i, t, att, d_send, d_recv).start()
+        spread(i, a_direct[i], att, d_send, d_recv)
 
     per_tp = seqs // n_tp
 
@@ -968,9 +1081,8 @@
     def output(i, cross):
         place = 1 - side if cross else side
         block = place * waves + i
-        for t in range(sources):
-            if targets[t][1] == cross:
-                spread_wait(i, t, att, d_send, d_recv)
+        if cross:
+            crossed(i, a_direct[i], *a_route)
         attended = jnp.concatenate([att[block, f] for f in range(n_far)], axis=1)
         term = dot(attended, out_w[...])
         for j in range(wave):
@@ -980,16 +1092,33 @@
             pl.when(tp != t)(e_copy(s, t).start)
 
     for i in range(waves):
-        for cross in range(2):
-            attend(i, cross)
-        if i > 0:
-            merge(i - 1)
-        tree(i)
-    merge(waves - 1)
+        pass_kv(i, 0)
+    pass_on(0, q_direct[0], *q_route)
+    attend(0, 0)
+    for i in range(waves):
+        if i + 1 < waves:
+            pass_on(i + 1, q_direct[i + 1], *q_route)
+            attend(i + 1, 0)
+        for step in range(1, len(strides)):
+            if 0 <= i - step + 1:
+                pass_kv(i - step + 1, step)
+        attend(i, 1)
+    for step in range(1, len(strides)):
+        for i in range(max(waves - step + 1, 0), waves):
+            pass_kv(i, step)
     load_of["out"].wait()
     for i in range(waves):
-        for cross in range(2):
-            output(i, cross)
+        tree(i)
+        if i >= 2:
+            pass_on(i - 2, a_direct[i - 2], *a_route)
+        merge(i)
+    if waves >= 2:
+        pass_on(waves - 2, a_direct[waves - 2], *a_route)
+    for i in range(waves):
+        if i == waves - 1:
+            pass_on(i, a_direct[i], *a_route)
+        output(i, 0)
+        output(i, 1)
 
     done = []
     for j in range(per_tp):
@@ -1007,16 +1136,22 @@
     out[...] = jnp.concatenate(done, axis=0).astype(BF16)
 
     for i in range(waves):
-        x_copy(i, q_out, q_in, qx_send, qx_recv).wait_send()
+        if i < waves - 1:
+            x_copy(i, q_out, q_in, qx_send, qx_recv).wait_send()
+            for d in range(1, n_far):
+                z_copy(i, d, q_own, q_far, qz_send, qz_recv).wait_send()
         x_copy(i, kv_out, kv_in, kx_send, kx_recv).wait_send()
-        for d in range(1, n_far):
-            z_copy(i, d, q_own, q_far, qz_send, qz_recv).wait_send()
-            z_copy(i, d, kv_pass, kv_far, kz_send, kz_recv).wait_send()
+        for st in strides:
+            for m in range(n_far // (2 * st)):
+                halve_copy(i, st, m).wait_send()
+        sent(i, q_direct[i], *q_route)
+        sent(i, a_direct[i], *a_route)
         for t in range(sources):
-            spread_copy(i, t, qbuf, b_send, b_recv).wait_send()
-            spread_copy(i, t, att, d_send, d_recv).wait_send()
             mix_copy(i, t, 0, mix, mix_in).wait_send()
             mix_copy(i, t, 1, stat, stat_in).wait_send()
+    for d in range(1, n_far):
+        last_copy(d).wait_send()
+    last_cross().wait_send()
     for s in range(seqs):
         t = s // per_tp
         pl.when(tp != t)(e_copy(s, t).wait_send)
@@ -1024,7 +1159,7 @@
 
 def wave_size(n, n_tp, seqs, props, heads, width):
     n_far = n // 2
-    if n % 2 or seqs % 2 or seqs % n_tp or heads % n_far or width % (n_far * LANES):
+    if n < 4 or n & (n - 1) or seqs % 2 or seqs % n_tp or heads % n_far or width % (n_far * LANES):
         return 0
     head_dim = width // heads
     own = heads // n_far
@@ -1072,9 +1207,11 @@
         if wave:
             n_far = n // 2
             waves = seqs // 2 // wave
+            q_waves = max(waves - 1, 1)
             wrows = wave * props
             wcols = width // n_far
             per_tp = seqs // n_tp
+            s_rows = max(4, 2 * (heads // n_far))
             block_q = (n_far, wrows + 8, wcols)
             block_kv = (n_far, 2 * wrows, wcols)
             body_of = functools.partial(by_heads, n, n_tp, wave)
@@ -1093,10 +1230,13 @@
                 pltpu.VMEM(cache_keys.shape, BF16),
                 pltpu.VMEM(cache_values.shape, BF16),
                 pltpu.VMEM((rows, 3 * depth), BF16),
-                pltpu.VMEM((waves,) + block_q, F32),
-                pltpu.VMEM((waves,) + block_q, F32),
-                pltpu.VMEM((waves,) + block_q, F32),
-                pltpu.VMEM((n_far - 1, waves) + block_q[1:], F32),
+                pltpu.VMEM((q_waves,) + block_q, F32),
+                pltpu.VMEM((q_waves,) + block_q, F32),
+                pltpu.VMEM((q_waves,) + block_q, F32),
+                pltpu.VMEM((n_far - 1, q_waves) + block_q[1:], F32),
+                pltpu.VMEM((n_far, 2) + block_q[1:], F32),
+                pltpu.VMEM((n_far - 1, 2) + block_q[1:], F32),
+                pltpu.VMEM(block_q[1:], F32),
                 pltpu.VMEM((waves,) + block_kv, BF16),
                 pltpu.VMEM((waves,) + block_kv, BF16),
                 pltpu.VMEM((waves,) + block_kv, F32),
@@ -1105,8 +1245,8 @@
                 pltpu.VMEM((2 * waves, n_far, wrows, wcols), BF16),
                 pltpu.VMEM((2 * waves, n_far, wrows, wcols), BF16),
                 pltpu.VMEM((n - 1, waves, wrows, wcols), BF16),
-                pltpu.VMEM((2 * waves, n_far, 8, LANES), F32),
-                pltpu.VMEM((n - 1, waves, 8, LANES), F32),
+                pltpu.VMEM((2 * waves, n_far, s_rows, LANES), F32),
+                pltpu.VMEM((n - 1, waves, s_rows, LANES), F32),
                 pltpu.VMEM((2 * waves, n_far, wrows, wcols), BF16),
                 pltpu.VMEM((seqs,) + folded, BF16),
                 pltpu.VMEM((n_tp - 1, per_tp) + folded, BF16),
@@ -1136,6 +1276,12 @@
                 dma((2 * waves, n_far)),
                 dma((seqs,)),
                 dma((n_tp - 1, per_tp)),
+                dma((waves,)),
+                dma((waves,)),
+                dma((waves,)),
+                dma((waves,)),
+                dma((n_far,)),
+                dma((n_far,)),
             ]
         else:
             body_of = functools.partial(by_sequence, n, n_tp)
@@ -1191,12 +1337,12 @@
             ]
         return pl.pallas_call(
             body_of,
-            out_shape=jax.ShapeDtypeStruct((block, cols), BF16),
+            out_shape=pltpu.VMEM((block, cols), BF16),
             in_specs=[hbm] * 13,
             out_specs=vmem,
             scratch_shapes=scratch,
             compiler_params=pltpu.CompilerParams(
-                collective_id=0, has_side_effects=True, vmem_limit_bytes=67_043_328
+                collective_id=0, has_side_effects=True, vmem_limit_bytes=67_043_328 - 131072
             ),
         )(
             tokens,

time: 57.6 us -> 47.1 us (0.82)
  Pallas kernels: 55.8 us -> 46.1 us
  local copies, waits for them, and re-layouts: 1.52 us -> 0.64 us
    pallas_call x1, Pallas kernels: 55.8 us -> 46.1 us  [body(): pl.pallas_call(body_of, out_shape=pltpu.VMEM((block, cols), BF16), in_spe...]
    unnamed x1, local copies, waits for them, and re-layouts: 1.52 us -> 0.64 us
where the time goes in v3:
time: 47.1 us; the launch traced here: 46.7 us
  Pallas kernels  46.1 us (98%)
  local copies, waits for them, and re-layouts  0.64 us (1%)
    pallas_call x1, Pallas kernels, body(): pl.pallas_call(body_of, out_shape=pltpu.VMEM((block, cols), BF16), in_spe...  46.1 us

profile of v3, /device:TPU:0, one launch (start us, length us, event | category | flops | bytes accessed | tf_op | source)
XLA Modules:
  0.0 46.7 jit_solution(12597313614072508659)
XLA Ops:
  0.0 46.1 %shard_map.127 = bf16[72,512]{1,0:T(8,128)(2,1)S(1)} custom-call(bf16[288,512]{1,0:T(8,128)(2,1)} %tokens_hbm.1, f32[1,512]{1,0:T(1,128)} %bitcast.4, bf16[512,512]{1,0:T(8,128)(2,1)} %query_hbm.1, bf16[512,512]{1,0:T(8,128)(2,1)} %key_hbm.1, bf16[512,512]{1,0:T(8,128)(2,1)} %value_hbm.1, bf16[32,4096]{1,0:T(8,128)(2,1)} %bitcast.3, f32[1,32]{1,0:T(1,128)} %bitcast.5, ...), custom_call_target="tpu_custom_call" | custom-call | tf_op jit(solution)/shard_map/pallas_call | solution.py:1338
  46.1 0.6 %copy.15 = bf16[72,512]{1,0:T(8,128)(2,1)} copy(bf16[72,512]{1,0:T(8,128)(2,1)S(1)} %shard_map.127) | data formatting | bytes 147456

commit v4 on v3

--- a/solution.py
+++ b/solution.py
@@ -865,6 +865,42 @@
     q_direct = [False] * waves
     a_direct = [i > 0 for i in range(waves)]
 
+    strides = [1 << b for b in range(n_far.bit_length() - 1)]
+
+    def halve_copy(i, st, m):
+        slot = sum(n_far // (2 * x) for x in strides if x < st) + m
+        partner = far + st - 2 * st * lax.rem(lax.div(far, st), 2)
+        return pltpu.make_async_remote_copy(
+            src_ref=kv_pass.at[i, lax.rem(partner, 2 * st) + 2 * st * m],
+            dst_ref=kv_far.at[slot, i],
+            send_sem=kz_send.at[slot, i],
+            recv_sem=kz_recv.at[slot, i],
+            device_id=near_id(partner, side),
+        )
+
+    def halve_start(i, st):
+        partner = far + st - 2 * st * lax.rem(lax.div(far, st), 2)
+        for m in range(n_far // (2 * st)):
+            f = lax.rem(partner, 2 * st) + 2 * st * m
+            kv_pass[i, f] = kv_own[i, f].astype(BF16)
+            halve_copy(i, st, m).start()
+
+    def halve_wait(i, st):
+        for m in range(n_far // (2 * st)):
+            halve_copy(i, st, m).wait_recv()
+            f = lax.rem(far, 2 * st) + 2 * st * m
+            slot = sum(n_far // (2 * x) for x in strides if x < st) + m
+            kv_own[i, f] = kv_own[i, f] + kv_far[slot, i].astype(F32)
+
+    def pass_kv(i, step):
+        if step:
+            halve_wait(i, strides[step - 1])
+        else:
+            x_copy(i, kv_out, kv_in, kx_send, kx_recv).wait_recv()
+            kv_own[i] = kv_own[i] + kv_in[i].astype(F32)
+        if step < len(strides):
+            halve_start(i, strides[step])
+
     lane8 = iota((8, LANES), 1)
     row8 = iota((8, LANES), 0)
 
@@ -892,42 +928,8 @@
 
     for i in range(waves):
         owner_q(i)
-
-    strides = [1 << b for b in range(n_far.bit_length() - 1)]
-
-    def halve_copy(i, st, m):
-        slot = sum(n_far // (2 * x) for x in strides if x < st) + m
-        partner = far + st - 2 * st * lax.rem(lax.div(far, st), 2)
-        return pltpu.make_async_remote_copy(
-            src_ref=kv_pass.at[i, lax.rem(partner, 2 * st) + 2 * st * m],
-            dst_ref=kv_far.at[slot, i],
-            send_sem=kz_send.at[slot, i],
-            recv_sem=kz_recv.at[slot, i],
-            device_id=near_id(partner, side),
-        )
-
-    def halve_start(i, st):
-        partner = far + st - 2 * st * lax.rem(lax.div(far, st), 2)
-        for m in range(n_far // (2 * st)):
-            f = lax.rem(partner, 2 * st) + 2 * st * m
-            kv_pass[i, f] = kv_own[i, f].astype(BF16)
-            halve_copy(i, st, m).start()
-
-    def halve_wait(i, st):
-        for m in range(n_far // (2 * st)):
-            halve_copy(i, st, m).wait_recv()
-            f = lax.rem(far, 2 * st) + 2 * st * m
-            slot = sum(n_far // (2 * x) for x in strides if x < st) + m
-            kv_own[i, f] = kv_own[i, f] + kv_far[slot, i].astype(F32)
-
-    def pass_kv(i, step):
-        if step:
-            halve_wait(i, strides[step - 1])
-        else:
-            x_copy(i, kv_out, kv_in, kx_send, kx_recv).wait_recv()
-            kv_own[i] = kv_own[i] + kv_in[i].astype(F32)
-        if step < len(strides):
-            halve_start(i, strides[step])
+        if i < waves - 1:
+            pass_kv(i, 0)
 
     group = min(heads, 256 // head_dim)
     gwidth = group * head_dim
@@ -1091,21 +1093,31 @@
             t = lax.div(s, per_tp)
             pl.when(tp != t)(e_copy(s, t).start)
 
-    for i in range(waves):
-        pass_kv(i, 0)
+    advanced = [0] * waves
+
+    def advance(count):
+        for i in range(waves):
+            if count and advanced[i] + 1 < len(strides):
+                advanced[i] += 1
+                pass_kv(i, advanced[i])
+                count -= 1
+
     pass_on(0, q_direct[0], *q_route)
     attend(0, 0)
-    for i in range(waves):
+    pass_kv(waves - 1, 0)
+    advance(1)
+    for i in range(1, waves):
+        pass_on(i, q_direct[i], *q_route)
+        if i == 1:
+            attend(1, 0)
+            advance(1)
+    attend(0, 1)
+    advance(1)
+    for i in range(1, waves):
         if i + 1 < waves:
-            pass_on(i + 1, q_direct[i + 1], *q_route)
             attend(i + 1, 0)
-        for step in range(1, len(strides)):
-            if 0 <= i - step + 1:
-                pass_kv(i - step + 1, step)
         attend(i, 1)
-    for step in range(1, len(strides)):
-        for i in range(max(waves - step + 1, 0), waves):
-            pass_kv(i, step)
+    advance(waves * len(strides))
     load_of["out"].wait()
     for i in range(waves):
         tree(i)

time: 47.1 us -> 46.5 us (0.987)
  no operation moved by 1% of the time
where the time goes in v4:
time: 46.5 us; the launch traced here: 46.3 us
  Pallas kernels  45.7 us (98%)
  local copies, waits for them, and re-layouts  0.64 us (1%)
    pallas_call x1, Pallas kernels, body(): pl.pallas_call(body_of, out_shape=pltpu.VMEM((block, cols), BF16), in_spe...  45.7 us

profile of v4, /device:TPU:0, one launch (start us, length us, event | category | flops | bytes accessed | tf_op | source)
XLA Modules:
  0.0 46.3 jit_solution(16903664388707082802)
XLA Ops:
  0.0 45.7 %shard_map.127 = bf16[72,512]{1,0:T(8,128)(2,1)S(1)} custom-call(bf16[288,512]{1,0:T(8,128)(2,1)} %tokens_hbm.1, f32[1,512]{1,0:T(1,128)} %bitcast.4, bf16[512,512]{1,0:T(8,128)(2,1)} %query_hbm.1, bf16[512,512]{1,0:T(8,128)(2,1)} %key_hbm.1, bf16[512,512]{1,0:T(8,128)(2,1)} %value_hbm.1, bf16[32,4096]{1,0:T(8,128)(2,1)} %bitcast.3, f32[1,32]{1,0:T(1,128)} %bitcast.5, ...), custom_call_target="tpu_custom_call" | custom-call | tf_op jit(solution)/shard_map/pallas_call | solution.py:1350
  45.7 0.6 %copy.15 = bf16[72,512]{1,0:T(8,128)(2,1)} copy(bf16[72,512]{1,0:T(8,128)(2,1)S(1)} %shard_map.127) | data formatting | bytes 147456

commit v5 on v4

--- a/solution.py
+++ b/solution.py
@@ -575,6 +575,11 @@
     inv_s,
     tmix,
     tstat,
+    held,
+    swap,
+    swap_in,
+    swap_stat,
+    swap_stat_in,
     widen,
     load_sem,
     cache_sem,
@@ -596,8 +601,8 @@
     e_recv,
     qr_send,
     qr_recv,
-    ar_send,
-    ar_recv,
+    s_send,
+    s_recv,
     l_send,
     l_recv,
 ):
@@ -861,9 +866,18 @@
             spread_wait(i, t, buf, send, recv)
 
     q_route = (qbuf, b_send, b_recv, qr_send, qr_recv)
-    a_route = (att, d_send, d_recv, ar_send, ar_recv)
+    zone = n_far // 2
+    place_in = lax.rem(far, zone)
+    zone_of = lax.div(far, zone)
+    near = [(d, 0) for d in range(1, zone)] + [(d, 1) for d in range(zone)]
+
+    def place_at(d):
+        return lax.rem(place_in + d, zone)
+
+    def zone_id(d, cross):
+        return near_id(zone_of * zone + place_at(d), 1 - side if cross else side)
+
     q_direct = [False] * waves
-    a_direct = [i > 0 for i in range(waves)]
 
     strides = [1 << b for b in range(n_far.bit_length() - 1)]
 
@@ -940,14 +954,14 @@
     position = iota((heads, pos_dev), 1) + me * pos_dev
 
     def mix_copy(i, t, which, src, dst):
-        d, cross = targets[t]
+        d, cross = near[t]
         block = (1 - side if cross else side) * waves + i
         return pltpu.make_async_remote_copy(
-            src_ref=src.at[block, far_id(d)],
+            src_ref=src.at[block, place_at(d)],
             dst_ref=dst.at[t, i],
             send_sem=c_send.at[which, t, i],
             recv_sem=c_recv.at[which, t, i],
-            device_id=target_id(d, cross),
+            device_id=zone_id(d, cross),
         )
 
     def attend(i, cross):
@@ -997,7 +1011,7 @@
         ]
         mixed = jnp.concatenate(mixes, axis=0).astype(BF16)
         for f in range(n_far):
-            mix[block, f] = mixed[:, f * cols : (f + 1) * cols]
+            mix[block, f % zone, f // zone] = mixed[:, f * cols : (f + 1) * cols]
         acc = jnp.zeros((wrows, LANES), F32)
         for h in range(heads):
             f, k = divmod(h, own_heads)
@@ -1006,9 +1020,9 @@
                 acc = jnp.where(lane_w == f * 8 + at, col, acc)
         flat = tile_rows(acc, LANES).T
         for f in range(n_far):
-            stat[block, f] = flat[f * 8 : f * 8 + stat.shape[2]]
-        for t in range(sources):
-            if targets[t][1] == cross:
+            stat[block, f % zone, f // zone] = flat[f * 8 : f * 8 + stat.shape[3]]
+        for t in range(len(near)):
+            if near[t][1] == cross:
                 mix_copy(i, t, 0, mix, mix_in).start()
                 mix_copy(i, t, 1, stat, stat_in).start()
 
@@ -1024,8 +1038,7 @@
         q = jnp.concatenate([jnp.where(own_head_of == h, q, 0.0) for h in range(own_heads)], axis=0)
         scores = dot_nt(q.astype(BF16), new_k) * scale
         path = path_s[i]
-        path_cols = tile_rows(path, LANES).T[:wrows]
-        shifts = [path_cols[:, h : h + 1] - path[h : h + 1] for h in range(own_heads)]
+        shifts = [jnp.broadcast_to(-path[h : h + 1], (wrows, LANES)) for h in range(own_heads)]
         scores = scores + jnp.concatenate(shifts, axis=0)
         live = jnp.concatenate([anc_s[i, :wrows]] * own_heads, axis=0) > 0.5
         scores = jnp.where(live, scores, LOW)
@@ -1043,30 +1056,84 @@
         tmix[i] = merged
         tstat[i] = tile_rows(acc, LANES).T[:8]
 
+    def swap_copy(i, which, src, dst):
+        return pltpu.make_async_remote_copy(
+            src_ref=src.at[i],
+            dst_ref=dst.at[i],
+            send_sem=s_send.at[which, i],
+            recv_sem=s_recv.at[which, i],
+            device_id=near_id((1 - zone_of) * zone + place_in, side),
+        )
+
+    def turn(tiles):
+        flat = jnp.concatenate([jnp.where(row8 < own_heads, x, 0.0) for x in tiles], axis=0)
+        turned = tile_rows(flat, LANES).T[:wrows]
+        high = turned.astype(BF16)
+        low = (turned - high.astype(F32)).astype(BF16)
+        both = jnp.concatenate([high, low], axis=1)
+        return dot(both, widen[:, : len(tiles) * cols])
+
+    def lift(st):
+        return pltpu.roll(st, 8 - own_heads, 0)
+
+    def weigh(wide, first, parts):
+        total = jnp.zeros((wrows, cols), F32)
+        for k, m in enumerate(parts):
+            at = (first + k) * cols
+            total = total + wide[:, at : at + cols] * m.astype(F32)
+        return total
+
     def merge(i):
         block = side * waves + i
-        for t in range(sources):
+        for t in range(len(near)):
             mix_copy(i, t, 0, mix, mix_in).wait_recv()
             mix_copy(i, t, 1, stat, stat_in).wait_recv()
-        stats = [stat[block, far]] + [stat_in[t, i] for t in range(sources)]
-        stats = [tile_rows(st, 8) for st in stats]
-        path = path_s[i]
-        tops = [st + path for st in stats] + [tstat[i]]
-        totals = [pltpu.roll(st, 8 - own_heads, 0) for st in stats + [tstat[i]]]
-        best = functools.reduce(jnp.maximum, tops)
-        factors = [jnp.exp(top - best) for top in tops]
-        denom = functools.reduce(jnp.add, [f * t for f, t in zip(factors, totals)])
-        factors = [jnp.where(row8 < own_heads, f / denom, 0.0) for f in factors]
-        turned = tile_rows(jnp.concatenate(factors, axis=0), LANES).T[:wrows]
-        high = turned.astype(BF16)
-        low = (turned - high.astype(F32)).astype(BF16)
-        wide = dot(jnp.concatenate([high, low], axis=1), widen[...])
-        mixes = [mix[block, far]] + [mix_in[t, i] for t in range(sources)] + [tmix[i]]
-        numer = jnp.zeros((wrows, cols), F32)
-        for k, m in enumerate(mixes):
-            numer = numer + wide[:, k * cols : (k + 1) * cols] * m.astype(F32)
-        att[block, far] = numer.astype(BF16)
-        spread(i, a_direct[i], att, d_send, d_recv)
+        tiles = []
+        for k in range(2):
+            stats = [stat[block, place_in, k]] + [stat_in[t, i, k] for t in range(len(near))]
+            stats = [tile_rows(st, 8) for st in stats]
+            absent = jnp.where(row8 < own_heads, LOW, 0.0)
+            stats.append(jnp.where(zone_of == k, tstat[i], absent))
+            best = functools.reduce(jnp.maximum, stats)
+            factors = [jnp.exp(st - best) for st in stats]
+            total = functools.reduce(jnp.add, [f * lift(st) for f, st in zip(factors, stats)])
+            packed = jnp.where(row8 < own_heads, best, pltpu.roll(total, own_heads, 0))
+            swap_stat[i, k] = packed[: swap_stat.shape[2]]
+            tiles += factors
+        wide = turn(tiles)
+        for k in range(2):
+            parts = [mix[block, place_in, k]] + [mix_in[t, i, k] for t in range(len(near))] + [tmix[i]]
+            held[i, k] = weigh(wide, k * len(parts), parts)
+            swap[i, k] = held[i, k].astype(BF16)
+        swap_copy(i, 0, swap, swap_in).start()
+        swap_copy(i, 1, swap_stat, swap_stat_in).start()
+
+    def att_copy(i, t, block, place):
+        d, cross = near[t]
+        return pltpu.make_async_remote_copy(
+            src_ref=att.at[block, place],
+            dst_ref=att.at[block, place],
+            send_sem=d_send.at[t, i],
+            recv_sem=d_recv.at[block, place],
+            device_id=zone_id(d, cross),
+        )
+
+    def finish(i):
+        block = side * waves + i
+        swap_copy(i, 0, swap, swap_in).wait_recv()
+        swap_copy(i, 1, swap_stat, swap_stat_in).wait_recv()
+        tiles = []
+        for k in range(2):
+            stats = [tile_rows(st[i, k], 8) for st in (swap_stat, swap_stat_in)]
+            best = jnp.maximum(stats[0], stats[1])
+            factors = [jnp.exp(st - best) for st in stats]
+            denom = functools.reduce(jnp.add, [f * lift(st) for f, st in zip(factors, stats)])
+            tiles += [f / denom for f in factors]
+        wide = turn(tiles)
+        for k in range(2):
+            att[block, place_in, k] = weigh(wide, 2 * k, (held[i, k], swap_in[i, k])).astype(BF16)
+        for t in range(len(near)):
+            att_copy(i, t, block, place_in).start()
 
     per_tp = seqs // n_tp
 
@@ -1083,9 +1150,10 @@
     def output(i, cross):
         place = 1 - side if cross else side
         block = place * waves + i
-        if cross:
-            crossed(i, a_direct[i], *a_route)
-        attended = jnp.concatenate([att[block, f] for f in range(n_far)], axis=1)
+        for t, (d, over) in enumerate(near):
+            if over == cross:
+                att_copy(i, t, block, place_at(d)).wait_recv()
+        attended = jnp.concatenate([att[block, f % zone, f // zone] for f in range(n_far)], axis=1)
         term = dot(attended, out_w[...])
         for j in range(wave):
             s = place * half_seqs + i * wave + j
@@ -1114,21 +1182,17 @@
     attend(0, 1)
     advance(1)
     for i in range(1, waves):
-        if i + 1 < waves:
-            attend(i + 1, 0)
         attend(i, 1)
+    for i in range(2, waves):
+        attend(i, 0)
     advance(waves * len(strides))
     load_of["out"].wait()
     for i in range(waves):
         tree(i)
-        if i >= 2:
-            pass_on(i - 2, a_direct[i - 2], *a_route)
         merge(i)
-    if waves >= 2:
-        pass_on(waves - 2, a_direct[waves - 2], *a_route)
     for i in range(waves):
-        if i == waves - 1:
-            pass_on(i, a_direct[i], *a_route)
+        finish(i)
+    for i in range(waves):
         output(i, 0)
         output(i, 1)
 
@@ -1157,8 +1221,10 @@
             for m in range(n_far // (2 * st)):
                 halve_copy(i, st, m).wait_send()
         sent(i, q_direct[i], *q_route)
-        sent(i, a_direct[i], *a_route)
-        for t in range(sources):
+        swap_copy(i, 0, swap, swap_in).wait_send()
+        swap_copy(i, 1, swap_stat, swap_stat_in).wait_send()
+        for t in range(len(near)):
+            att_copy(i, t, side * waves + i, place_in).wait_send()
             mix_copy(i, t, 0, mix, mix_in).wait_send()
             mix_copy(i, t, 1, stat, stat_in).wait_send()
     for d in range(1, n_far):
@@ -1175,7 +1241,7 @@
         return 0
     head_dim = width // heads
     own = heads // n_far
-    if own > 4 or 8 * (n + 1) > LANES or (heads % min(heads, max(256 // head_dim, 1))):
+    if own > 4 or 16 * (n_far + 1) > LANES or (heads % min(heads, max(256 // head_dim, 1))):
         return 0
     for wave in range(1, seqs // 2 + 1):
         fits = wave * props % 16 == 0 and wave * props <= LANES
@@ -1220,6 +1286,7 @@
             n_far = n // 2
             waves = seqs // 2 // wave
             q_waves = max(waves - 1, 1)
+            zone = n_far // 2
             wrows = wave * props
             wcols = width // n_far
             per_tp = seqs // n_tp
@@ -1255,11 +1322,11 @@
                 pltpu.VMEM((waves,) + block_kv, BF16),
                 pltpu.VMEM((n_far - 1, waves) + block_kv[1:], BF16),
                 pltpu.VMEM((2 * waves, n_far, wrows, wcols), BF16),
-                pltpu.VMEM((2 * waves, n_far, wrows, wcols), BF16),
-                pltpu.VMEM((n - 1, waves, wrows, wcols), BF16),
-                pltpu.VMEM((2 * waves, n_far, s_rows, LANES), F32),
-                pltpu.VMEM((n - 1, waves, s_rows, LANES), F32),
-                pltpu.VMEM((2 * waves, n_far, wrows, wcols), BF16),
+                pltpu.VMEM((2 * waves, zone, 2, wrows, wcols), BF16),
+                pltpu.VMEM((n_far - 1, waves, 2, wrows, wcols), BF16),
+                pltpu.VMEM((2 * waves, zone, 2, s_rows, LANES), F32),
+                pltpu.VMEM((n_far - 1, waves, 2, s_rows, LANES), F32),
+                pltpu.VMEM((2 * waves, zone, 2, wrows, wcols), BF16),
                 pltpu.VMEM((seqs,) + folded, BF16),
                 pltpu.VMEM((n_tp - 1, per_tp) + folded, BF16),
                 pltpu.VMEM((-(-seqs // 8) * 8, LANES), jnp.int32),
@@ -1269,7 +1336,12 @@
                 pltpu.VMEM((waves, wrows, wcols), F32),
                 pltpu.VMEM((waves, wrows, wcols), F32),
                 pltpu.VMEM((waves, 8, LANES), F32),
-                pltpu.VMEM((2 * LANES, (n + 1) * wcols), BF16),
+                pltpu.VMEM((waves, 2, wrows, wcols), F32),
+                pltpu.VMEM((waves, 2, wrows, wcols), BF16),
+                pltpu.VMEM((waves, 2, wrows, wcols), BF16),
+                pltpu.VMEM((waves, 2, s_rows, LANES), F32),
+                pltpu.VMEM((waves, 2, s_rows, LANES), F32),
+                pltpu.VMEM((2 * LANES, 2 * (n_far + 1) * wcols), BF16),
                 dma((11,)),
                 dma((2, seqs)),
                 dma((waves,)),
@@ -1282,16 +1354,16 @@
                 dma((n_far - 1, waves)),
                 dma((n - 1, waves)),
                 dma((2 * waves, n_far)),
-                dma((2, n - 1, waves)),
-                dma((2, n - 1, waves)),
-                dma((n - 1, waves)),
-                dma((2 * waves, n_far)),
+                dma((2, n_far - 1, waves)),
+                dma((2, n_far - 1, waves)),
+                dma((n_far - 1, waves)),
+                dma((2 * waves, zone)),
                 dma((seqs,)),
                 dma((n_tp - 1, per_tp)),
                 dma((waves,)),
                 dma((waves,)),
-                dma((waves,)),
-                dma((waves,)),
+                dma((2, waves)),
+                dma((2, waves)),
                 dma((n_far,)),
                 dma((n_far,)),
             ]

time: 46.5 us -> 45.2 us (0.972)
  the two profiles are of different devices: /device:TPU:0 before, /device:TPU:1 now
where the time goes in v5:
time: 45.2 us; the launch traced here: 45.1 us
  Pallas kernels  44.4 us (98%)
  local copies, waits for them, and re-layouts  0.64 us (1%)
    pallas_call x1, Pallas kernels, body(): pl.pallas_call(body_of, out_shape=pltpu.VMEM((block, cols), BF16), in_spe...  44.4 us

profile of v5, /device:TPU:1, one launch (start us, length us, event | category | flops | bytes accessed | tf_op | source)
XLA Modules:
  0.0 45.1 jit_solution(8012672125922187745)
XLA Ops:
  0.0 44.4 %shard_map.127 = bf16[72,512]{1,0:T(8,128)(2,1)S(1)} custom-call(bf16[288,512]{1,0:T(8,128)(2,1)} %tokens_hbm.1, f32[1,512]{1,0:T(1,128)} %bitcast.4, bf16[512,512]{1,0:T(8,128)(2,1)} %query_hbm.1, bf16[512,512]{1,0:T(8,128)(2,1)} %key_hbm.1, bf16[512,512]{1,0:T(8,128)(2,1)} %value_hbm.1, bf16[32,4096]{1,0:T(8,128)(2,1)} %bitcast.3, f32[1,32]{1,0:T(1,128)} %bitcast.5, ...), custom_call_target="tpu_custom_call" | custom-call | tf_op jit(solution)/shard_map/pallas_call | solution.py:1422
  44.4 0.6 %copy.15 = bf16[72,512]{1,0:T(8,128)(2,1)} copy(bf16[72,512]{1,0:T(8,128)(2,1)S(1)} %shard_map.127) | data formatting | bytes 147456

commit v6 on v5

--- a/solution.py
+++ b/solution.py
@@ -1182,9 +1182,10 @@
     attend(0, 1)
     advance(1)
     for i in range(1, waves):
+        if i == waves - 1:
+            for k in range(2, waves):
+                attend(k, 0)
         attend(i, 1)
-    for i in range(2, waves):
-        attend(i, 0)
     advance(waves * len(strides))
     load_of["out"].wait()
     for i in range(waves):

time: 45.2 us -> 44.7 us (0.989)
  the two profiles are of different devices: /device:TPU:1 before, /device:TPU:0 now
where the time goes in v6:
time: 44.7 us; the launch traced here: 44.6 us
  Pallas kernels  44 us (98%)
  local copies, waits for them, and re-layouts  0.64 us (1%)
    pallas_call x1, Pallas kernels, body(): pl.pallas_call(body_of, out_shape=pltpu.VMEM((block, cols), BF16), in_spe...  44 us

profile of v6, /device:TPU:0, one launch (start us, length us, event | category | flops | bytes accessed | tf_op | source)
XLA Modules:
  0.0 44.6 jit_solution(2194864045980155014)
XLA Ops:
  0.0 44.0 %shard_map.127 = bf16[72,512]{1,0:T(8,128)(2,1)S(1)} custom-call(bf16[288,512]{1,0:T(8,128)(2,1)} %tokens_hbm.1, f32[1,512]{1,0:T(1,128)} %bitcast.4, bf16[512,512]{1,0:T(8,128)(2,1)} %query_hbm.1, bf16[512,512]{1,0:T(8,128)(2,1)} %key_hbm.1, bf16[512,512]{1,0:T(8,128)(2,1)} %value_hbm.1, bf16[32,4096]{1,0:T(8,128)(2,1)} %bitcast.3, f32[1,32]{1,0:T(1,128)} %bitcast.5, ...), custom_call_target="tpu_custom_call" | custom-call | tf_op jit(solution)/shard_map/pallas_call | solution.py:1423
  44.0 0.6 %copy.15 = bf16[72,512]{1,0:T(8,128)(2,1)} copy(bf16[72,512]{1,0:T(8,128)(2,1)S(1)} %shard_map.127) | data formatting | bytes 147456

commit v7 on v6

--- a/solution.py
+++ b/solution.py
@@ -877,7 +877,7 @@
     def zone_id(d, cross):
         return near_id(zone_of * zone + place_at(d), 1 - side if cross else side)
 
-    q_direct = [False] * waves
+    q_direct = [i == waves - 1 for i in range(waves)]
 
     strides = [1 << b for b in range(n_far.bit_length() - 1)]
 

time: 44.7 us -> 44.7 us (level)
  no operation moved by 1% of the time
where the time goes in v7:
time: 44.7 us; the launch traced here: 44.5 us
  Pallas kernels  43.9 us (98%)
  local copies, waits for them, and re-layouts  0.64 us (1%)
    pallas_call x1, Pallas kernels, body(): pl.pallas_call(body_of, out_shape=pltpu.VMEM((block, cols), BF16), in_spe...  43.9 us

profile of v7, /device:TPU:0, one launch (start us, length us, event | category | flops | bytes accessed | tf_op | source)
XLA Modules:
  0.0 44.5 jit_solution(14781701929483151404)
XLA Ops:
  0.0 43.9 %shard_map.127 = bf16[72,512]{1,0:T(8,128)(2,1)S(1)} custom-call(bf16[288,512]{1,0:T(8,128)(2,1)} %tokens_hbm.1, f32[1,512]{1,0:T(1,128)} %bitcast.4, bf16[512,512]{1,0:T(8,128)(2,1)} %query_hbm.1, bf16[512,512]{1,0:T(8,128)(2,1)} %key_hbm.1, bf16[512,512]{1,0:T(8,128)(2,1)} %value_hbm.1, bf16[32,4096]{1,0:T(8,128)(2,1)} %bitcast.3, f32[1,32]{1,0:T(1,128)} %bitcast.5, ...), custom_call_target="tpu_custom_call" | custom-call | tf_op jit(solution)/shard_map/pallas_call | solution.py:1423
  43.9 0.6 %copy.15 = bf16[72,512]{1,0:T(8,128)(2,1)} copy(bf16[72,512]{1,0:T(8,128)(2,1)S(1)} %shard_map.127) | data formatting | bytes 147456
